TPU v7x, 32 devices: a whole 2x2x4 slice. The times are simulated.
32 devices in a mesh: rep: 2 (over x), fs: 8 (over z, y), tp: 2 (over core).
Axes of the slice: x: 2, y: 2, z: 4, core: 2. Of those that a mesh axis runs over, the one named last changes fastest.
Arguments:
- inputs_next: bfloat16 [2048, 2048], P(('rep', 'fs'), 'tp'), parts along dimension 0, may hold values from -6 to 6
- inputs_prev: bfloat16 [2048, 2048], P(('rep', 'fs'), 'tp'), parts along dimension 0, may hold values from -6 to 6
- hidden_prev: bfloat16 [2048, 8192], P(('rep', 'fs')), parts along dimension 0, may hold values from -6 to 6
- cotangent: bfloat16 [2048, 2048], P(('rep', 'fs'), 'tp'), parts along dimension 0, may hold values from -6 to 6
- up_weight: bfloat16 [2048, 8192], P('tp', 'fs'), may hold values from -0.125 to 0.125
- down_weight: bfloat16 [8192, 2048], P('fs', 'tp'), may hold values from -0.0625 to 0.0625
- up_accum: float32 [4096, 8192], P(('rep', 'tp'), 'fs'), parts along dimension 0, may hold values from -192 to 192
- down_accum: float32 [16384, 2048], P(('rep', 'fs'), 'tp'), parts along dimension 0, may hold values from -192 to 192
Outputs:
- output_next: bfloat16 [2048, 2048], P(('rep', 'fs'), 'tp'), parts along dimension 0
- hidden_next: bfloat16 [2048, 8192], P(('rep', 'fs')), parts along dimension 0
- input_grad: bfloat16 [2048, 2048], P(('rep', 'fs'), 'tp'), parts along dimension 0
- up_accum_out: float32 [4096, 8192], P(('rep', 'tp'), 'fs'), parts along dimension 0
- down_accum_out: float32 [16384, 2048], P(('rep', 'fs'), 'tp'), parts along dimension 0
There are 2 independent parts, one for each index of `rep`. A program takes and returns all parts, laid end to end along the dimension named above; an argument that names none is the same for every part. Nothing has to cross between parts.
All inputs are finite; a program needn't handle non-finite values.
Results may differ from a plain program's by a relative error of at most 0.034.
Values may be sent and summed in bfloat16 or wider, within the bound.
No kernel may reach another device: no remote copies, remote signals or barrier semaphores. Data moves between devices by JAX's collectives and lax.ppermute only.
A program may use at most 128 MiB of HBM per device.

v0:
```python
import jax
import jax.numpy as jnp
from jax import lax
from jax.sharding import PartitionSpec as P


def squared_relu(values):
    return jnp.square(jax.nn.relu(values.astype(jnp.float32))).astype(jnp.bfloat16)


def contract(left, right, left_dim, right_dim):
    return lax.dot_general(
        left, right, (((left_dim,), (right_dim,)), ((), ())), preferred_element_type=jnp.float32
    )


def local(
    inputs_next, inputs_prev, hidden_prev, cotangent, up_weight, down_weight, up_accum, down_accum
):
    up_whole = lax.all_gather(up_weight, "fs", axis=1, tiled=True)
    hidden_terms = jnp.dot(inputs_next, up_whole, preferred_element_type=jnp.float32).astype(
        jnp.bfloat16
    )
    hidden_next = lax.psum(hidden_terms, "tp").astype(jnp.float32).astype(jnp.bfloat16)
    acts_next = squared_relu(hidden_next)
    saved_inputs, cotangent_all = (
        lax.all_gather(inputs_prev, "fs", axis=0, tiled=True),
        lax.all_gather(cotangent, "fs", axis=0, tiled=True),
    )
    acts_rows = lax.all_to_all(acts_next, "fs", split_axis=1, concat_axis=0, tiled=True)
    output_next = lax.psum_scatter(
        jnp.dot(acts_rows, down_weight, preferred_element_type=jnp.float32).astype(jnp.bfloat16),
        "fs",
        scatter_dimension=0,
        tiled=True,
    )
    saved_spread = lax.all_to_all(hidden_prev, "fs", split_axis=1, concat_axis=0, tiled=True)
    acts_spread = squared_relu(saved_spread)
    back_terms = contract(cotangent_all, down_weight, 1, 1).astype(jnp.bfloat16)
    back_sum = lax.psum(back_terms, "tp").astype(jnp.float32)
    grad_spread = (back_sum * 2.0 * jax.nn.relu(saved_spread.astype(jnp.float32))).astype(
        jnp.bfloat16
    )
    hidden_grad = lax.all_to_all(grad_spread, "fs", split_axis=0, concat_axis=1, tiled=True)
    input_grad = contract(hidden_grad, up_whole, 1, 1).astype(jnp.bfloat16)
    up_accum_out = up_accum + contract(saved_inputs, grad_spread, 0, 0)
    down_accum_out = down_accum + contract(acts_spread, cotangent_all, 0, 0)
    return (output_next, hidden_next, input_grad, up_accum_out, down_accum_out)


def solution(mesh):
    return jax.shard_map(
        local,
        mesh=mesh,
        in_specs=(
            P(("rep", "fs"), "tp"),
            P(("rep", "fs"), "tp"),
            P(("rep", "fs"), None),
            P(("rep", "fs"), "tp"),
            P("tp", "fs"),
            P("fs", "tp"),
            P(("rep", "tp"), "fs"),
            P(("rep", "fs"), "tp"),
        ),
        out_specs=(
            P(("rep", "fs"), "tp"),
            P(("rep", "fs"), None),
            P(("rep", "fs"), "tp"),
            P(("rep", "tp"), "fs"),
            P(("rep", "fs"), "tp"),
        ),
        check_vma=False,
    )
```

profile of v0, /device:TPU:0, one launch (start us, length us, event | category | flops | bytes accessed | tf_op | source)
XLA Modules:
  0.0 542.0 jit_solution(11550131855770351500)
XLA Ops:
  7.2 0.0 copy-start
  7.2 0.0 all-gather.6.cloned.1.call-start
  7.2 0.7 all-gather.6.cloned.1.call-update
  7.9 0.0 all-gather.4.cloned.1.call-start
  8.0 0.7 all-gather.4.cloned.1.call-update
  8.7 0.0 copy-start.5
  8.7 0.0 all-reduce.3.cloned.1.call-start
  8.7 53.2 %all-gather.6.cloned.1.call-done = bf16[1024,1024]{1,0:T(8,128)(2,1)} async-done(((bf16[128,1024]{1,0:T(8,128)(2,1)}), bf16[1024,1024]{1,0:T(8,128)(2,1)}) %all-gather.6.cloned.1.call-update) | async-done | bytes 2097168 | tf_op jit(solution)/shard_map/all_gather | solution.py:28
  62.0 0.0 copy-done
  62.0 5.3 convolution_convert_fusion.1
  67.2 222.7 %all-gather.4.cloned.1.call-done = bf16[1024,8192]{1,0:T(8,128)(2,1)} async-done(((bf16[1024,1024]{1,0:T(8,128)(2,1)}), bf16[1024,8192]{1,0:T(8,128)(2,1)}) %all-gather.4.cloned.1.call-update) | async-done | bytes 16777232 | tf_op jit(solution)/shard_map/all_gather | solution.py:20
  290.0 0.0 copy-done.5
  290.0 9.4 %convolution_convert_fusion = bf16[128,8192]{1,0:T(8,128)(2,1)} fusion(bf16[128,1024]{1,0:T(8,128)(2,1)S(1)} %copy-done.5, bf16[1024,8192]{1,0:T(8,128)(2,1)} %all-gather.4.cloned.1.call-done), kind=kOutput, calls=%fused_computation | convolution fusion | flops 2148532224 | bytes 19136512 | tf_op jit(solution)/shard_map/dot_general | solution.py:21
  299.4 0.0 all-reduce.3.cloned.1.call-update
  299.4 3.2 copy.25
  302.6 4.3 all-to-all-start.1
  306.9 19.2 %all-reduce.3.cloned.1.call-done = (bf16[128,8192]{1,0:T(8,128)(2,1)}, bf16[1024,1024]{1,0:T(8,128)(2,1)}) async-done(((bf16[128,8192]{1,0:T(8,128)(2,1)}, bf16[1024,1024]{1,0:T(8,128)(2,1)}), (bf16[128,8192]{1,0:T(8,128)(2,1)}, bf16[1024,1024]{1,0:T(8,128)(2,1)})) %all-reduce.3.cloned.1.call-update) | async-done | bytes 4194320 | tf_op jit(solution)/shard_map/psum | solution.py:24
  326.1 2.1 multiply_convert_fusion
  328.2 1.5 copy.26
  329.7 25.1 %all-to-all-done.1 = bf16[128,8,1024]{2,0,1:T(8,128)(2,1)} async-done(((bf16[128,8,1024]{2,0,1:T(8,128)(2,1)}), bf16[128,8,1024]{2,0,1:T(8,128)(2,1)}, u32[]{:S(2)}, u32[]{:S(2)}) %all-to-all-start.1) | async-done | bytes 2097184 | tf_op jit(solution)/shard_map/all_to_all | solution.py:37
  354.8 4.4 all-to-all-start
  359.2 0.0 all-gather.8.cloned.1.call-start
  359.2 0.5 all-gather.8.cloned.1.call-update
  359.8 0.0 copy-start.3
  359.8 2.3 convert_maximum_fusion
  362.1 0.0 copy-done.3
  362.1 3.2 fusion.1
  365.3 3.9 copy.18
  369.2 59.6 %all-to-all-done = bf16[128,8,1024]{2,0,1:T(8,128)(2,1)} async-done(((bf16[128,8,1024]{2,0,1:T(8,128)(2,1)}), bf16[128,8,1024]{2,0,1:T(8,128)(2,1)}, u32[]{:S(2)}, u32[]{:S(2)}) %all-to-all-start) | async-done | bytes 2097184 | tf_op jit(solution)/shard_map/all_to_all | solution.py:30
  428.8 4.3 all-to-all-start.2
  433.1 0.2 reduce-scatter.2.cloned.1.call-start
  433.4 5.2 convolution_convert_fusion.2
  438.6 0.0 reduce-scatter.2.cloned.1.call-update
  438.6 0.0 copy-start.2
  438.6 5.5 %copy.19 = f32[1024,1024]{0,1:T(8,128)} copy(f32[1024,1024]{1,0:T(8,128)} %param.14) | data formatting | bytes 8388608 | tf_op args[6]
  444.1 0.0 all-gather.8.cloned.1.call-done
  444.1 0.0 copy-done.2
  444.1 7.2 %bitcast_add_fusion = f32[1024,1024]{0,1:T(8,128)} fusion(f32[1024,1024]{0,1:T(8,128)} %copy.19, bf16[1024,1024]{1,0:T(8,128)(2,1)S(1)} %copy-done.2, bf16[1024,1024]{1,0:T(8,128)(2,1)} %all-gather.8.cloned.1.call-done), kind=kOutput, calls=%fused_computation.5 | convolution fusion | flops 2148532224 | bytes 12582912 | tf_op jit(solution)/shard_map/dot_general | solution.py:12
  451.4 0.0 copy-start.4
  451.4 5.5 %copy.20 = f32[1024,1024]{1,0:T(8,128)} copy(f32[1024,1024]{0,1:T(8,128)} %bitcast_add_fusion) | data formatting | bytes 8388608
  456.9 0.0 copy-done.4
  456.9 7.3 %convolution_add_fusion = f32[1024,1024]{1,0:T(8,128)} fusion(f32[1024,1024]{1,0:T(8,128)} %param.15, bf16[1024,1024]{1,0:T(8,128)(2,1)S(1)} %copy-done.4, bf16[1024,1024]{1,0:T(8,128)(2,1)} %all-gather.6.cloned.1.call-done), kind=kOutput, calls=%fused_computation.10 | convolution fusion | flops 2148532224 | bytes 12582912 | tf_op jit(solution)/shard_map/dot_general | solution.py:12
  464.1 32.6 %all-to-all-done.2 = bf16[8,128,1024]{1,2,0:T(8,128)(2,1)} async-done(((bf16[8,128,1024]{1,2,0:T(8,128)(2,1)}), bf16[8,128,1024]{1,2,0:T(8,128)(2,1)}, u32[]{:S(2)}, u32[]{:S(2)}) %all-to-all-start.2) | async-done | bytes 2097184 | tf_op jit(solution)/shard_map/all_to_all | solution.py:44
  496.7 0.0 copy-start.1
  496.7 13.1 %convolution_convert_fusion.3 = bf16[128,1024]{1,0:T(8,128)(2,1)} fusion(bf16[128,8192]{0,1:T(8,128)(2,1)} %bitcast.6, bf16[1024,8192]{1,0:T(8,128)(2,1)} %all-gather.4.cloned.1.call-done), kind=kOutput, calls=%fused_computation.13 | convolution fusion | flops 2147614720 | bytes 19136512 | tf_op jit(solution)/shard_map/dot_general | solution.py:12
  509.8 22.5 %reduce-scatter.2.cloned.1.call-done = bf16[128,1024]{1,0:T(8,128)(2,1)} async-done(((bf16[1024,1024]{1,0:T(8,128)(2,1)}), bf16[128,1024]{1,0:T(8,128)(2,1)}) %reduce-scatter.2.cloned.1.call-update) | async-done | bytes 262160 | tf_op jit(solution)/shard_map/reduce_scatter | solution.py:31
  532.3 3.1 copy.29
  535.4 0.0 copy-done.1
Async XLA Ops:
  7.2 54.8 %copy-start = (bf16[1024,1024]{1,0:T(8,128)(2,1)S(1)}, bf16[1024,1024]{1,0:T(8,128)(2,1)}, u32[]{:S(2)}) copy-start(bf16[1024,1024]{1,0:T(8,128)(2,1)} %param.13) | copy-start | bytes 6291460
  7.2 54.8 %all-gather.6.cloned.1.call-start = ((), (), s32[]{:S(2)}) async-start(), calls=%async_computation.6 | async-start | bytes 2359296 | tf_op jit(solution)/shard_map/all_gather | solution.py:28
  7.9 282.1 %all-gather.4.cloned.1.call-start = ((), (), s32[]{:S(2)}) async-start(), calls=%async_computation.4 | async-start | bytes 18874368 | tf_op jit(solution)/shard_map/all_gather | solution.py:20
  8.7 281.3 %copy-start.5 = (bf16[128,1024]{1,0:T(8,128)(2,1)S(1)}, bf16[128,1024]{1,0:T(8,128)(2,1)}, u32[]{:S(2)}) copy-start(bf16[128,1024]{1,0:T(8,128)(2,1)} %param.8) | copy-start | bytes 786436
  8.7 317.5 %all-reduce.3.cloned.1.call-start = ((), (), s32[]{:S(2)}) async-start(), calls=%async_computation.8 | async-start | bytes 8388608 | tf_op jit(solution)/shard_map/psum | solution.py:24
  302.6 52.2 %all-to-all-start.1 = ((bf16[128,8,1024]{2,0,1:T(8,128)(2,1)}), bf16[128,8,1024]{2,0,1:T(8,128)(2,1)}, u32[]{:S(2)}, u32[]{:S(2)}) async-start(bf16[128,8,1024]{2,0,1:T(8,128)(2,1)} %bitcast.40), calls=%async_computation.2 | async-start | bytes 4194304 | tf_op jit(solution)/shard_map/all_to_all | solution.py:37
  354.8 74.0 %all-to-all-start = ((bf16[128,8,1024]{2,0,1:T(8,128)(2,1)}), bf16[128,8,1024]{2,0,1:T(8,128)(2,1)}, u32[]{:S(2)}, u32[]{:S(2)}) async-start(bf16[128,8,1024]{2,0,1:T(8,128)(2,1)} %bitcast.39), calls=%async_computation | async-start | bytes 4194304 | tf_op jit(solution)/shard_map/all_to_all | solution.py:30
  359.2 84.9 %all-gather.8.cloned.1.call-start = ((), (), s32[]{:S(2)}) async-start(), calls=%async_computation.7 | async-start | bytes 2359296 | tf_op jit(solution)/shard_map/all_gather | solution.py:27
  359.8 2.3 copy-start.3
  428.8 67.9 %all-to-all-start.2 = ((bf16[8,128,1024]{1,2,0:T(8,128)(2,1)}), bf16[8,128,1024]{1,2,0:T(8,128)(2,1)}, u32[]{:S(2)}, u32[]{:S(2)}) async-start(bf16[8,128,1024]{1,2,0:T(8,128)(2,1)} %copy.18), calls=%async_computation.3 | async-start | bytes 4194304 | tf_op jit(solution)/shard_map/all_to_all | solution.py:44
  433.1 99.2 %reduce-scatter.2.cloned.1.call-start = ((), (), s32[]{:S(2)}) async-start(), calls=%async_computation.5 | async-start | bytes 2359296 | tf_op jit(solution)/shard_map/reduce_scatter | solution.py:31
  438.6 5.5 %copy-start.2 = (bf16[1024,1024]{1,0:T(8,128)(2,1)S(1)}, bf16[1024,1024]{1,0:T(8,128)(2,1)}, u32[]{:S(2)}) copy-start(bf16[1024,1024]{1,0:T(8,128)(2,1)} %get-tuple-element.18) | copy-start | bytes 6291460
  451.4 5.5 %copy-start.4 = (bf16[1024,1024]{1,0:T(8,128)(2,1)S(1)}, bf16[1024,1024]{1,0:T(8,128)(2,1)}, u32[]{:S(2)}) copy-start(bf16[1024,1024]{1,0:T(8,128)(2,1)} %get-tuple-element.17) | copy-start | bytes 6291460
  496.7 38.7 %copy-start.1 = (bf16[1024,1024]{1,0:T(8,128)(2,1)S(1)}, bf16[1024,1024]{1,0:T(8,128)(2,1)}, u32[]{:S(2)}) copy-start(bf16[1024,1024]{1,0:T(8,128)(2,1)} %param.13) | copy-start | bytes 6291460
Sparse Core Ops, SparseCore 0:
  10.1 51.7 all-gather.5
  64.1 225.7 all-gather.3
  299.6 26.5 all-reduce.2
  361.8 70.7 all-gather.7
  438.7 93.5 reduce-scatter.1
where the time goes:
time: 543 us; the launch traced here: 542 us
  waiting for transfers between devices  437 us (80%)
  matrix products  47.6 us (9%)
  local copies, waits for them, and re-layouts  22.7 us (4%)
  between operations  13.9 us (3%)
  starting transfers between devices  13.4 us (2%)
  other arithmetic  7.57 us (1%)
    all_gather x1, waiting for transfers between devices, local(): up_whole = lax.all_gather(up_weight, 'fs', axis=1, tiled=True)  223 us
    all_to_all x1, waiting for transfers between devices, local(): lax.all_to_all(acts_next, 'fs', split_axis=1, concat_axis=0, tiled=True)  59.6 us
    all_gather x1, waiting for transfers between devices, local(): lax.all_gather(cotangent, 'fs', axis=0, tiled=True)  53.2 us
    dot_general x4, matrix products, contract(): lax.dot_general(left, right, (((left_dim,), (right_dim,)), ((), ())), pre...  32.9 us
    all_to_all x1, waiting for transfers between devices, local(): lax.all_to_all(grad_spread, 'fs', split_axis=0, concat_axis=1, tiled=True)  32.6 us
    all_to_all x1, waiting for transfers between devices, local(): lax.all_to_all(hidden_prev, 'fs', split_axis=1, concat_axis=0, tiled=True)  25.1 us
    reduce_scatter x1, waiting for transfers between devices, local(): lax.psum_scatter(jnp.dot(acts_rows, down_weight, preferred_element_type=j...  22.5 us
    psum x1, waiting for transfers between devices, local(): lax.psum(hidden_terms, 'tp').astype(jnp.float32).astype(jnp.bfloat16)  19.2 us
  transfers between devices with their start and end apart: 8, of which 7 were waited for; matrix products, arithmetic and copies ran while one was open for 12% of the time, Pallas kernels for 0%

commit v1 on v0

v1 whole, which is shorter than its diff:
```python
import jax
import jax.numpy as jnp
from jax import lax
from jax.sharding import PartitionSpec as P


def squared_relu(values):
    return jnp.square(jax.nn.relu(values.astype(jnp.float32))).astype(jnp.bfloat16)


def contract(left, right, left_dim, right_dim):
    return lax.dot_general(
        left, right, (((left_dim,), (right_dim,)), ((), ())), preferred_element_type=jnp.float32
    )


def total_over_tp(terms, n_tp):
    if n_tp == 2:
        theirs = lax.ppermute(terms, "tp", [(0, 1), (1, 0)])
        return terms.astype(jnp.float32) + theirs.astype(jnp.float32)
    return lax.psum(terms, "tp").astype(jnp.float32)


def join_over_tp(part, n_tp):
    if n_tp == 2:
        theirs = lax.ppermute(part, "tp", [(0, 1), (1, 0)])
        first = lax.axis_index("tp") == 0
        return jnp.stack(
            [jnp.where(first, part, theirs), jnp.where(first, theirs, part)], axis=part.ndim - 1
        )
    return lax.all_gather(part, "tp", axis=part.ndim - 1, tiled=False)


def make_local(n_fs, n_tp):
    def local(
        inputs_next, inputs_prev, hidden_prev, cotangent, up_weight, down_weight, up_accum, down_accum
    ):
        me_tp = lax.axis_index("tp")
        rows, ff = hidden_prev.shape
        units = ff // n_fs
        piece = units // n_tp

        def gather(x):
            return lax.all_gather(x, "fs", axis=0, tiled=True)

        inputs_all = gather(inputs_next)
        cotangent_all = gather(cotangent)
        saved_inputs = gather(inputs_prev)

        saved_mine = lax.dynamic_slice_in_dim(
            hidden_prev.reshape(rows, n_fs, n_tp, piece), me_tp, 1, axis=2
        ).reshape(rows, n_fs, piece)
        saved_mine = lax.all_to_all(saved_mine, "fs", split_axis=1, concat_axis=0, tiled=True)
        saved_spread = join_over_tp(saved_mine.reshape(n_fs * rows, piece), n_tp)
        saved_spread = saved_spread.reshape(n_fs * rows, units)

        hidden_terms = contract(inputs_all, up_weight, 1, 0).astype(jnp.bfloat16)
        hidden_spread = total_over_tp(hidden_terms, n_tp).astype(jnp.bfloat16)
        hidden_mine = lax.dynamic_slice_in_dim(hidden_spread, me_tp * piece, piece, axis=1)
        hidden_mine = lax.all_to_all(
            hidden_mine.reshape(n_fs, rows, piece), "fs", split_axis=0, concat_axis=0, tiled=True
        )
        hidden_next = join_over_tp(hidden_mine, n_tp)
        hidden_next = jnp.transpose(hidden_next, (1, 0, 2, 3)).reshape(rows, ff)
        output_terms = contract(squared_relu(hidden_spread), down_weight, 1, 0).astype(jnp.bfloat16)
        output_next = lax.psum_scatter(output_terms, "fs", scatter_dimension=0, tiled=True)

        back_terms = contract(cotangent_all, down_weight, 1, 1).astype(jnp.bfloat16)
        back_sum = total_over_tp(back_terms, n_tp)
        grad_spread = (back_sum * 2.0 * jax.nn.relu(saved_spread.astype(jnp.float32))).astype(
            jnp.bfloat16
        )
        input_terms = contract(grad_spread, up_weight, 1, 1).astype(jnp.bfloat16)
        input_grad = lax.psum_scatter(input_terms, "fs", scatter_dimension=0, tiled=True)
        down_accum_out = down_accum + contract(squared_relu(saved_spread), cotangent_all, 0, 0)
        up_accum_out = up_accum + contract(saved_inputs, grad_spread, 0, 0)
        return (output_next, hidden_next, input_grad, up_accum_out, down_accum_out)

    return local


def solution(mesh):
    return jax.shard_map(
        make_local(mesh.shape["fs"], mesh.shape["tp"]),
        mesh=mesh,
        in_specs=(
            P(("rep", "fs"), "tp"),
            P(("rep", "fs"), "tp"),
            P(("rep", "fs"), None),
            P(("rep", "fs"), "tp"),
            P("tp", "fs"),
            P("fs", "tp"),
            P(("rep", "tp"), "fs"),
            P(("rep", "fs"), "tp"),
        ),
        out_specs=(
            P(("rep", "fs"), "tp"),
            P(("rep", "fs"), None),
            P(("rep", "fs"), "tp"),
            P(("rep", "tp"), "fs"),
            P(("rep", "fs"), "tp"),
        ),
        check_vma=False,
    )
```

time: 543 us -> 335 us (0.62)
  waiting for transfers between devices: 437 us -> 240 us
  matrix products: 47.6 us -> 33.5 us
    all_gather x3, waiting for transfers between devices: 276 us -> 74.8 us  [gather(): return lax.all_gather(x, 'fs', axis=0, tiled=True)]
    reduce_scatter x1 -> x2, waiting for transfers between devices: 22.5 us -> 119 us  [the longest x1 71.4 us: local(): lax.psum_scatter(output_terms, 'fs', scatter_dimension=0, tiled=True)]
    all_to_all x3 -> x2, waiting for transfers between devices: 117 us -> 34.3 us  [the longest x1 34.3 us: local(): lax.all_to_all(hidden_mine.reshape(n_fs, rows, piece), 'fs', split_axis=0...]
    psum x1 -> x0, waiting for transfers between devices: 19.2 us -> none  [local(): lax.psum(hidden_terms, 'tp').astype(jnp.float32).astype(jnp.bfloat16)]
    dot_general x2 -> x0, matrix products: 14.7 us -> none  [the longest x1 9.44 us: local(): jnp.dot(inputs_next, up_whole, preferred_element_type=jnp.float32)]
    ppermute x0 -> x4, waiting for transfers between devices: none -> 9.64 us  [the longest x2 5.49 us: join_over_tp(): theirs = lax.ppermute(part, 'tp', [(0, 1), (1, 0)])]
    all_to_all x3 -> x0, local copies, waits for them, and re-layouts: 8.56 us -> none  [the longest x1 3.92 us: local(): lax.all_to_all(grad_spread, 'fs', split_axis=0, concat_axis=1, tiled=True)]
    unnamed x15 -> x14, local copies, waits for them, and re-layouts: 14.1 us -> 20.4 us
  transfers between devices with their start and end apart: 8 -> 11, of which waited for: 7 -> 7; matrix products, arithmetic and copies ran while one was open for 12% -> 20% of each run, Pallas kernels for 0% -> 0%
where the time goes in v1:
time: 335 us
  waiting for transfers between devices  240 us (72%)
  matrix products  33.5 us (10%)
  local copies, waits for them, and re-layouts  26.9 us (8%)
  between operations  13.9 us (4%)
  starting transfers between devices  11.8 us (4%)
  other arithmetic  8.29 us (2%)
    all_gather x3, waiting for transfers between devices, gather(): return lax.all_gather(x, 'fs', axis=0, tiled=True)  74.8 us
    reduce_scatter x1, waiting for transfers between devices, local(): lax.psum_scatter(output_terms, 'fs', scatter_dimension=0, tiled=True)  71.4 us
    reduce_scatter x1, waiting for transfers between devices, local(): lax.psum_scatter(input_terms, 'fs', scatter_dimension=0, tiled=True)  47.9 us
    all_to_all x1, waiting for transfers between devices, local(): lax.all_to_all(hidden_mine.reshape(n_fs, rows, piece), 'fs', split_axis=0...  34.3 us
    dot_general x6, matrix products, contract(): lax.dot_general(left, right, (((left_dim,), (right_dim,)), ((), ())), pre...  33.5 us
    unnamed x14, local copies, waits for them, and re-layouts  20.4 us
    all_to_all x1, starting transfers between devices, local(): lax.all_to_all(saved_mine, 'fs', split_axis=1, concat_axis=0, tiled=True)  7.31 us
  transfers between devices with their start and end apart: 11, of which 7 were waited for; matrix products, arithmetic and copies ran while one was open for 20% of the time, Pallas kernels for 0%

profile of v1, /device:TPU:0, one launch (start us, length us, event | category | flops | bytes accessed | tf_op | source)
XLA Modules:
  0.0 334.6 jit_solution(10980953622583183163)
XLA Ops:
  7.2 0.0 copy-start
  7.2 0.0 all-gather.6.cloned.1.call-start
  7.2 0.7 all-gather.6.cloned.1.call-update
  7.9 0.0 all-gather.4.cloned.1.call-start
  8.0 0.7 all-gather.4.cloned.1.call-update
  8.7 4.1 %copy.29 = bf16[128,8192]{0,1:T(8,128)(2,1)} copy(bf16[128,8192]{1,0:T(8,128)(2,1)} %param.10) | data formatting | bytes 4194304 | tf_op args[2]
  12.7 1.3 dynamic-slice_bitcast_fusion
  14.0 1.3 copy.31
  15.4 7.3 %all-to-all-start.1 = ((bf16[128,8,512]{2,0,1:T(8,128)(2,1)}), bf16[128,8,512]{2,0,1:T(8,128)(2,1)S(1)}, u32[]{:S(2)}, u32[]{:S(2)}) async-start(bf16[128,8,512]{2,0,1:T(8,128)(2,1)} %copy.31), calls=%async_computation.2 | async-start | bytes 2097152 | tf_op jit(solution)/shard_map/all_to_all | solution.py:53
  22.7 0.0 all-gather.8.cloned.1.call-start
  22.7 0.7 all-gather.8.cloned.1.call-update
  23.4 0.0 reduce-scatter.5.cloned.1.call-start
  23.4 49.5 %all-gather.6.cloned.1.call-done = bf16[1024,1024]{1,0:T(8,128)(2,1)} async-done(((bf16[128,1024]{1,0:T(8,128)(2,1)}), bf16[1024,1024]{1,0:T(8,128)(2,1)}) %all-gather.6.cloned.1.call-update) | async-done | bytes 2097168 | tf_op jit(solution)/shard_map/all_gather | solution.py:44
  72.9 5.9 %convolution_convert_fusion.1 = bf16[1024,1024]{1,0:T(8,128)(2,1)} fusion(bf16[1024,1024]{1,0:T(8,128)(2,1)} %all-gather.6.cloned.1.call-done, bf16[1024,1024]{1,0:T(8,128)(2,1)} %param.13), kind=kOutput, calls=%fused_computation.13 | convolution fusion | flops 2148532224 | bytes 6291456 | tf_op jit(solution)/shard_map/dot_general | solution.py:12
  78.8 0.0 collective-permute-start.2
  78.8 0.0 all-to-all-done.1
  78.8 0.5 collective-permute-start.3
  79.3 5.5 %collective-permute-done.3 = bf16[1024,512]{1,0:T(8,128)(2,1)} collective-permute-done((bf16[1024,512]{1,0:T(8,128)(2,1)S(1)}, bf16[1024,512]{1,0:T(8,128)(2,1)}, u32[]{:S(2)}, u32[]{:S(2)}) %collective-permute-start.3) | collective-permute-done | bytes 1048608 | tf_op jit(solution)/shard_map/ppermute | solution.py:26
  84.8 1.4 select_bitcast_fusion.1
  86.2 0.6 maximum_bitcast_fusion
  86.8 0.4 copy.38
  87.3 5.1 %multiply_convert_fusion.1 = bf16[1024,1024]{1,0:T(8,128)(2,1)S(1)} fusion(f32[1024,1024]{1,0:T(8,128)S(1)} %bitcast.37, bf16[1024,1024]{1,0:T(8,128)(2,1)} %collective-permute-done.2, bf16[1024,1024]{1,0:T(8,128)(2,1)} %convolution_convert_fusion.1), kind=kLoop, calls=%fused_computation.2 | loop fusion | flops 6291456 | bytes 10485760 | tf_op jit(solution)/shard_map/convert_element_type | solution.py:70
  92.3 0.0 copy-start.3
  92.3 1.3 copy-done.3
  93.6 3.8 %convolution_convert_fusion = bf16[1024,1024]{1,0:T(8,128)(2,1)} fusion(bf16[1024,1024]{1,0:T(8,128)(2,1)S(1)} %multiply_convert_fusion.1, bf16[1024,1024]{1,0:T(8,128)(2,1)S(1)} %copy-done), kind=kOutput, calls=%fused_computation.12 | convolution fusion | flops 2148532224 | bytes 6291456 | tf_op jit(solution)/shard_map/dot_general | solution.py:12
  97.4 0.0 reduce-scatter.5.cloned.1.call-update
  97.4 0.2 reduce-scatter.3.cloned.1.call-start
  97.7 25.4 %all-gather.4.cloned.1.call-done = bf16[1024,1024]{1,0:T(8,128)(2,1)} async-done(((bf16[128,1024]{1,0:T(8,128)(2,1)}), bf16[1024,1024]{1,0:T(8,128)(2,1)}) %all-gather.4.cloned.1.call-update) | async-done | bytes 2097168 | tf_op jit(solution)/shard_map/all_gather | solution.py:44
  123.0 3.9 %convolution_convert_fusion.2 = bf16[1024,1024]{1,0:T(8,128)(2,1)S(1)} fusion(bf16[1024,1024]{1,0:T(8,128)(2,1)} %all-gather.4.cloned.1.call-done, bf16[1024,1024]{1,0:T(8,128)(2,1)S(1)} %copy-done), kind=kOutput, calls=%fused_computation.14 | convolution fusion | flops 2148532224 | bytes 6291456 | tf_op jit(solution)/shard_map/dot_general | solution.py:12
  127.0 0.0 copy-start.4
  127.0 0.1 collective-permute-start
  127.0 4.1 %collective-permute-done = bf16[1024,1024]{1,0:T(8,128)(2,1)S(1)} collective-permute-done((bf16[1024,1024]{1,0:T(8,128)(2,1)S(1)}, bf16[1024,1024]{1,0:T(8,128)(2,1)S(1)}, u32[]{:S(2)}, u32[]{:S(2)}) %collective-permute-start) | collective-permute-done | bytes 2097184 | tf_op jit(solution)/shard_map/ppermute | solution.py:19
  131.2 1.0 add_convert_fusion
  132.2 3.7 %fusion.4 = bf16[1024,1024]{1,0:T(8,128)(2,1)} fusion(bf16[1024,1024]{1,0:T(8,128)(2,1)S(1)} %copy-done.4, bf16[1024,1024]{1,0:T(8,128)(2,1)S(1)} %add_convert_fusion), kind=kOutput, calls=%fused_computation.11 | convolution fusion | flops 2152726528 | bytes 6291456 | tf_op jit(solution)/shard_map/dot_general | solution.py:12
  135.9 0.0 reduce-scatter.3.cloned.1.call-update
  135.9 1.1 constant_dynamic-slice_fusion
  137.0 3.6 %all-to-all-start = ((bf16[8,128,512]{2,1,0:T(8,128)(2,1)}), bf16[8,128,512]{2,1,0:T(8,128)(2,1)S(1)}, u32[]{:S(2)}, u32[]{:S(2)}) async-start(bf16[8,128,512]{2,1,0:T(8,128)(2,1)} %bitcast), calls=%async_computation.1 | async-start | bytes 2097152 | tf_op jit(solution)/shard_map/all_to_all | solution.py:60
  140.5 5.4 %copy.33 = f32[1024,1024]{0,1:T(8,128)} copy(f32[1024,1024]{1,0:T(8,128)} %param.14) | data formatting | bytes 8388608 | tf_op args[6]
  145.9 34.3 %all-to-all-done = bf16[8,128,512]{2,1,0:T(8,128)(2,1)S(1)} async-done(((bf16[8,128,512]{2,1,0:T(8,128)(2,1)}), bf16[8,128,512]{2,1,0:T(8,128)(2,1)S(1)}, u32[]{:S(2)}, u32[]{:S(2)}) %all-to-all-start) | async-done | bytes 1048608 | tf_op jit(solution)/shard_map/all_to_all | solution.py:60
  180.2 8.5 %fusion.3 = f32[1024,1024]{1,0:T(8,128)} fusion(f32[1024,1024]{1,0:T(8,128)} %param.15, bf16[1024,1024]{1,0:T(8,128)(2,1)} %all-gather.6.cloned.1.call-done, f32[1024,1024]{1,0:T(8,128)} %bitcast.38), kind=kOutput, calls=%fused_computation.10 | convolution fusion | flops 2150629376 | bytes 14680064 | tf_op jit(solution)/shard_map/dot_general | solution.py:12
  188.7 7.8 %bitcast_add_fusion = f32[1024,1024]{0,1:T(8,128)} fusion(f32[1024,1024]{0,1:T(8,128)} %copy.33, bf16[1024,1024]{1,0:T(8,128)(2,1)} %copy-done.3, bf16[1024,1024]{1,0:T(8,128)(2,1)} %all-gather.8.cloned.1.call-done), kind=kOutput, calls=%fused_computation | convolution fusion | flops 2148532224 | bytes 12582912 | tf_op jit(solution)/shard_map/dot_general | solution.py:12
  196.5 5.3 %copy.35 = f32[1024,1024]{1,0:T(8,128)} copy(f32[1024,1024]{0,1:T(8,128)} %bitcast_add_fusion) | data formatting | bytes 8388608
  201.8 0.1 select_bitcast_fusion.3
  202.0 0.2 maximum_bitcast_fusion.1
  202.2 2.4 copy.28
  204.5 4.2 %copy.34 = bf16[128,8192]{1,0:T(8,128)(2,1)} copy(bf16[128,8192]{0,1:T(8,128)(2,1)} %bitcast.39) | data formatting | bytes 4194304
  208.8 47.9 %reduce-scatter.5.cloned.1.call-done = bf16[128,1024]{1,0:T(8,128)(2,1)} async-done(((bf16[1024,1024]{1,0:T(8,128)(2,1)}), bf16[128,1024]{1,0:T(8,128)(2,1)}) %reduce-scatter.5.cloned.1.call-update) | async-done | bytes 262160 | tf_op jit(solution)/shard_map/reduce_scatter | solution.py:74
  256.7 71.4 %reduce-scatter.3.cloned.1.call-done = bf16[128,1024]{1,0:T(8,128)(2,1)} async-done(((bf16[1024,1024]{1,0:T(8,128)(2,1)}), bf16[128,1024]{1,0:T(8,128)(2,1)}) %reduce-scatter.3.cloned.1.call-update) | async-done | bytes 262160 | tf_op jit(solution)/shard_map/reduce_scatter | solution.py:66
  (10 shorter events, 0.0 us)
Async XLA Ops:
  7.2 86.5 %copy-start = (bf16[1024,1024]{1,0:T(8,128)(2,1)S(1)}, bf16[1024,1024]{1,0:T(8,128)(2,1)}, u32[]{:S(2)}) copy-start(bf16[1024,1024]{1,0:T(8,128)(2,1)} %param.12) | copy-start | bytes 6291460
  7.2 65.7 %all-gather.6.cloned.1.call-start = ((), (), s32[]{:S(2)}) async-start(), calls=%async_computation.6 | async-start | bytes 2359296 | tf_op jit(solution)/shard_map/all_gather | solution.py:44
  7.9 115.1 %all-gather.4.cloned.1.call-start = ((), (), s32[]{:S(2)}) async-start(), calls=%async_computation.4 | async-start | bytes 2359296 | tf_op jit(solution)/shard_map/all_gather | solution.py:44
  15.4 63.5 %all-to-all-start.1 = ((bf16[128,8,512]{2,0,1:T(8,128)(2,1)}), bf16[128,8,512]{2,0,1:T(8,128)(2,1)S(1)}, u32[]{:S(2)}, u32[]{:S(2)}) async-start(bf16[128,8,512]{2,0,1:T(8,128)(2,1)} %copy.31), calls=%async_computation.2 | async-start | bytes 2097152 | tf_op jit(solution)/shard_map/all_to_all | solution.py:53
  22.7 166.0 %all-gather.8.cloned.1.call-start = ((), (), s32[]{:S(2)}) async-start(), calls=%async_computation.8 | async-start | bytes 2359296 | tf_op jit(solution)/shard_map/all_gather | solution.py:44
  23.4 233.3 %reduce-scatter.5.cloned.1.call-start = ((), (), s32[]{:S(2)}) async-start(), calls=%async_computation.7 | async-start | bytes 2359296 | tf_op jit(solution)/shard_map/reduce_scatter | solution.py:74
  78.8 8.4 %collective-permute-start.2 = (bf16[1024,1024]{1,0:T(8,128)(2,1)}, bf16[1024,1024]{1,0:T(8,128)(2,1)}, u32[]{:S(2)}, u32[]{:S(2)}) collective-permute-start(bf16[1024,1024]{1,0:T(8,128)(2,1)} %convolution_convert_fusion.1), channel_id=1, source_target_pairs={{0,1},{1,0},{2,3},{3,2},{4,5},{5,4},{6,7},{7,6},{8,9},{9,8},{10,11... | collective-permute-start | bytes 6291464 | tf_op jit(solution)/shard_map/ppermute | solution.py:19
  78.8 6.0 %collective-permute-start.3 = (bf16[1024,512]{1,0:T(8,128)(2,1)S(1)}, bf16[1024,512]{1,0:T(8,128)(2,1)}, u32[]{:S(2)}, u32[]{:S(2)}) collective-permute-start(bf16[1024,512]{1,0:T(8,128)(2,1)S(1)} %bitcast.41), channel_id=1, source_target_pairs={{0,1},{1,0},{2,3},{3,2},{4,5},{5,4},{6,7},{7,6},{8,9},{9,8},{10,11... | collective-permute-start | bytes 3145736 | tf_op jit(solution)/shard_map/ppermute | solution.py:26
  87.2 5.1 %copy-start.2 = (f32[2,128,8,512]{3,2,0,1:T(8,128)}, f32[2,128,8,512]{3,2,0,1:T(8,128)S(1)}, u32[]{:S(2)}) copy-start(f32[2,128,8,512]{3,2,0,1:T(8,128)S(1)} %copy.38) | copy-start | bytes 12582916
  92.3 1.3 copy-start.3
  97.4 230.6 %reduce-scatter.3.cloned.1.call-start = ((), (), s32[]{:S(2)}) async-start(), calls=%async_computation.5 | async-start | bytes 2359296 | tf_op jit(solution)/shard_map/reduce_scatter | solution.py:66
  127.0 5.2 %copy-start.4 = (bf16[1024,1024]{1,0:T(8,128)(2,1)S(1)}, bf16[1024,1024]{1,0:T(8,128)(2,1)}, u32[]{:S(2)}) copy-start(bf16[1024,1024]{1,0:T(8,128)(2,1)} %param.13) | copy-start | bytes 6291460
  127.0 4.2 %collective-permute-start = (bf16[1024,1024]{1,0:T(8,128)(2,1)S(1)}, bf16[1024,1024]{1,0:T(8,128)(2,1)S(1)}, u32[]{:S(2)}, u32[]{:S(2)}) collective-permute-start(bf16[1024,1024]{1,0:T(8,128)(2,1)S(1)} %convolution_convert_fusion.2), channel_id=1, source_target_pairs={{0,1},{1,0},{2,3},{3,2},{4,5},{5,4},{6,7},{7,6},{8,9},{9,8},{10,11... | collective-permute-start | bytes 6291464 | tf_op jit(solution)/shard_map/ppermute | solution.py:19
  137.0 43.2 %all-to-all-start = ((bf16[8,128,512]{2,1,0:T(8,128)(2,1)}), bf16[8,128,512]{2,1,0:T(8,128)(2,1)S(1)}, u32[]{:S(2)}, u32[]{:S(2)}) async-start(bf16[8,128,512]{2,1,0:T(8,128)(2,1)} %bitcast), calls=%async_computation.1 | async-start | bytes 2097152 | tf_op jit(solution)/shard_map/all_to_all | solution.py:60
  180.2 21.6 %collective-permute-start.1 = (bf16[8,128,512]{2,1,0:T(8,128)(2,1)S(1)}, bf16[8,128,512]{2,1,0:T(8,128)(2,1)S(1)}, u32[]{:S(2)}, u32[]{:S(2)}) collective-permute-start(bf16[8,128,512]{2,1,0:T(8,128)(2,1)S(1)} %all-to-all-done), channel_id=1, source_target_pairs={{0,1},{1,0},{2,3},{3,2},{4,5},{5,4},{6,7},{7,6},{8,9},{9,8},{10,11... | collective-permute-start | bytes 3145736 | tf_op jit(solution)/shard_map/ppermute | solution.py:26
  204.5 123.5 %copy-start.1 = (bf16[1024,1024]{1,0:T(8,128)(2,1)S(1)}, bf16[1024,1024]{1,0:T(8,128)(2,1)}, u32[]{:S(2)}) copy-start(bf16[1024,1024]{1,0:T(8,128)(2,1)} %param.12) | copy-start | bytes 6291460
Sparse Core Ops, SparseCore 0:
  10.1 62.7 all-gather.5
  75.0 47.9 all-gather.3
  125.2 59.9 all-gather.7
  189.1 67.5 reduce-scatter.4
  260.6 67.3 reduce-scatter.2

commit v2 on v1

v2 whole, which is shorter than its diff:
```python
import functools

import jax
import jax.numpy as jnp
from jax import lax
from jax.experimental import pallas as pl
from jax.experimental.pallas import tpu as pltpu
from jax.sharding import PartitionSpec as P


def contract(left, right, left_dim, right_dim):
    return lax.dot_general(
        left, right, (((left_dim,), (right_dim,)), ((), ())), preferred_element_type=jnp.float32
    )


def ring_order(mesh):
    n = mesh.shape["fs"]
    at = mesh.axis_names.index("fs")
    line = [mesh.devices[tuple(i if a == at else 0 for a in range(mesh.devices.ndim))] for i in range(n)]
    width = 2
    spots = [getattr(d, "coords", None) for d in line]
    if n > 2 and all(s is not None for s in spots):
        fast = [c for c in range(3) if spots[0][c] != spots[1][c]]
        if len(fast) == 1:
            width = len({s[fast[0]] for s in spots})
    if n % width or (n // width) % 2:
        width = 2
    order = [row * width for row in range(n // width)]
    for back, row in enumerate(reversed(range(n // width))):
        columns = list(range(1, width))
        order += [row * width + c for c in (columns if back % 2 == 0 else reversed(columns))]
    return order


def add_terms(*terms):
    total = terms[0].astype(jnp.float32)
    for term in terms[1:]:
        total = total + term.astype(jnp.float32)
    return total.astype(jnp.bfloat16)


class Ring:
    def __init__(self, order):
        self.n = n = len(order)
        self.order = order
        self.ahead = [(order[i], order[(i + 1) % n]) for i in range(n)]
        self.behind = [(b, a) for a, b in self.ahead]

    def shift(self, x, k):
        n, order = self.n, self.order
        return lax.ppermute(x, "fs", [(order[i], order[(i + k) % n]) for i in range(n)])

    def places(self):
        n = self.n
        place = [0] * n
        for i, index in enumerate(self.order):
            place[index] = i
        mine = jnp.asarray(place, jnp.int32)[lax.axis_index("fs")]
        return jnp.asarray(self.order, jnp.int32)[(mine + jnp.arange(n, dtype=jnp.int32)) % n]

    def gather(self, x):
        n, half = self.n, x.shape[0] // 2
        blocks = [x] + [None] * (n - 1)
        up = down = x
        for k in range(1, n // 2):
            up = lax.ppermute(up, "fs", self.ahead)
            down = lax.ppermute(down, "fs", self.behind)
            blocks[n - k], blocks[k] = up, down
        blocks[n // 2] = jnp.concatenate(
            [lax.ppermute(up[:half], "fs", self.ahead), lax.ppermute(down[half:], "fs", self.behind)]
        )
        return blocks

    def exchange(self, blocks):
        n = self.n
        return [blocks[0]] + [self.shift(blocks[n - j], n - j) for j in range(1, n)]

    def scatter_sum(self, blocks):
        n = self.n
        far = blocks[n // 2]
        half = far.shape[1] // 2
        up = lax.ppermute(far[:, :half], "fs", self.ahead)
        down = lax.ppermute(far[:, half:], "fs", self.behind)
        for k in range(n // 2 - 1, 0, -1):
            mine_up, mine_down = blocks[k], blocks[n - k]
            if k == n // 2 - 1:
                up = jnp.concatenate([add_terms(mine_up[:, :half], up), mine_up[:, half:]], axis=1)
                down = jnp.concatenate(
                    [mine_down[:, :half], add_terms(mine_down[:, half:], down)], axis=1
                )
            else:
                up, down = add_terms(mine_up, up), add_terms(mine_down, down)
            up = lax.ppermute(up, "fs", self.ahead)
            down = lax.ppermute(down, "fs", self.behind)
        return add_terms(blocks[0], up, down)


def pick_kernel(at_ref, x_ref, o_ref):
    o_ref[...] = x_ref[...]


def pick_columns(x, at, width):
    rows, count = x.shape[0], at.shape[0]
    if width % 128:
        cut = jnp.take(x.reshape(rows, -1, width), at, axis=1)
        return jnp.transpose(cut, (1, 0, 2)).reshape(count * rows, width)
    return pl.pallas_call(
        pick_kernel,
        out_shape=jax.ShapeDtypeStruct((count * rows, width), x.dtype),
        grid_spec=pltpu.PrefetchScalarGridSpec(
            num_scalar_prefetch=1,
            grid=(count,),
            in_specs=[pl.BlockSpec((rows, width), lambda i, at: (0, at[i]))],
            out_specs=pl.BlockSpec((rows, width), lambda i, at: (i, 0)),
        ),
        name="pick_columns",
    )(at, x)


def place_kernel(count, at_ref, *refs):
    o_ref = refs[count]
    for i in range(count):

        @pl.when(pl.program_id(0) == i)
        def _():
            o_ref[...] = refs[i][...]


def place_columns(parts, at, total):
    rows, width = parts[0].shape
    count = len(parts)
    return pl.pallas_call(
        functools.partial(place_kernel, count),
        out_shape=jax.ShapeDtypeStruct((rows, total), parts[0].dtype),
        grid_spec=pltpu.PrefetchScalarGridSpec(
            num_scalar_prefetch=1,
            grid=(count,),
            in_specs=[pl.BlockSpec((rows, width), lambda i, at: (0, 0))] * count,
            out_specs=pl.BlockSpec((rows, width), lambda i, at: (0, at[i])),
        ),
        name="place_columns",
    )(at, *parts)


def swap_tp(x):
    return lax.ppermute(x, "tp", [(0, 1), (1, 0)])


def total_over_tp(terms, n_tp):
    if n_tp == 2:
        return terms.astype(jnp.float32) + swap_tp(terms).astype(jnp.float32)
    return lax.psum(terms, "tp").astype(jnp.float32)


def squared_relu(values):
    return jnp.square(jax.nn.relu(values.astype(jnp.float32))).astype(jnp.bfloat16)


def make_local(ring, n_tp):
    n = ring.n

    def local(
        inputs_next, inputs_prev, hidden_prev, cotangent, up_weight, down_weight, up_accum, down_accum
    ):
        me_tp = lax.axis_index("tp")
        rows, ff = hidden_prev.shape
        units = ff // n
        piece = units // n_tp
        places = ring.places()

        def block(x, j):
            return lax.slice_in_dim(x, j * rows, (j + 1) * rows, axis=0)

        inputs_all = jnp.concatenate(ring.gather(inputs_next))
        cotangent_all = jnp.concatenate(ring.gather(cotangent))

        saved_out = pick_columns(hidden_prev, places * n_tp + me_tp, piece)
        saved_mine = jnp.concatenate(ring.exchange([block(saved_out, j) for j in range(n)]))
        if n_tp == 2:
            saved_theirs = swap_tp(saved_mine)
            first = me_tp == 0
            saved = jnp.concatenate(
                [
                    jnp.where(first, saved_mine, saved_theirs),
                    jnp.where(first, saved_theirs, saved_mine),
                ],
                axis=1,
            )
        else:
            saved = lax.all_gather(saved_mine, "tp", axis=1, tiled=True)

        hidden_terms = contract(inputs_all, up_weight, 1, 0).astype(jnp.bfloat16)
        hidden = total_over_tp(hidden_terms, n_tp).astype(jnp.bfloat16)
        hidden_mine = lax.dynamic_slice_in_dim(hidden, me_tp * piece, piece, axis=1)
        hidden_mine = ring.exchange([block(hidden_mine, j) for j in range(n)])
        if n_tp == 2:
            theirs = swap_tp(jnp.concatenate(hidden_mine))
            parts = hidden_mine + [block(theirs, j) for j in range(n)]
            at = jnp.concatenate([places * 2 + me_tp, places * 2 + 1 - me_tp])
        else:
            whole = lax.all_gather(jnp.concatenate(hidden_mine), "tp", axis=0, tiled=True)
            parts = [block(whole, j) for j in range(n * n_tp)]
            at = (places[None, :] * n_tp + jnp.arange(n_tp, dtype=jnp.int32)[:, None]).reshape(-1)
        if piece % 128 == 0:
            hidden_next = place_columns(parts, at, ff)
        else:
            stacked = jnp.stack(parts, axis=1)
            hidden_next = stacked[:, jnp.argsort(at), :].reshape(rows, ff)
        output_terms = contract(squared_relu(hidden), down_weight, 1, 0).astype(jnp.bfloat16)
        output_next = ring.scatter_sum([block(output_terms, j) for j in range(n)])

        back_terms = contract(cotangent_all, down_weight, 1, 1).astype(jnp.bfloat16)
        back_sum = total_over_tp(back_terms, n_tp)
        grad = (back_sum * 2.0 * jax.nn.relu(saved.astype(jnp.float32))).astype(jnp.bfloat16)
        input_terms = contract(grad, up_weight, 1, 1).astype(jnp.bfloat16)
        input_grad = ring.scatter_sum([block(input_terms, j) for j in range(n)])
        down_accum_out = down_accum + contract(squared_relu(saved), cotangent_all, 0, 0)
        saved_inputs = jnp.concatenate(ring.gather(inputs_prev))
        up_accum_out = up_accum + contract(saved_inputs, grad, 0, 0)
        return (output_next, hidden_next, input_grad, up_accum_out, down_accum_out)

    return local


def solution(mesh):
    return jax.shard_map(
        make_local(Ring(ring_order(mesh)), mesh.shape["tp"]),
        mesh=mesh,
        in_specs=(
            P(("rep", "fs"), "tp"),
            P(("rep", "fs"), "tp"),
            P(("rep", "fs"), None),
            P(("rep", "fs"), "tp"),
            P("tp", "fs"),
            P("fs", "tp"),
            P(("rep", "tp"), "fs"),
            P(("rep", "fs"), "tp"),
        ),
        out_specs=(
            P(("rep", "fs"), "tp"),
            P(("rep", "fs"), None),
            P(("rep", "fs"), "tp"),
            P(("rep", "tp"), "fs"),
            P(("rep", "fs"), "tp"),
        ),
        check_vma=False,
    )
```

time: 335 us -> 215 us (0.64)
  waiting for transfers between devices: 240 us -> 48.4 us
  starting transfers between devices: 11.8 us -> 104 us
  matrix products: 33.5 us -> 18.8 us
  Pallas kernels: 0 us -> 14 us
  between operations: 13.9 us -> 1.38 us
  local copies, waits for them, and re-layouts: 26.9 us -> 22.1 us
    reduce_scatter x2 -> x0, waiting for transfers between devices: 119 us -> none  [the longest x1 71.4 us: local(): lax.psum_scatter(output_terms, 'fs', scatter_dimension=0, tiled=True)]
    ppermute x4 -> x58, starting transfers between devices: 0.58 us -> 104 us  [the longest x14 30.7 us: shift(): lax.ppermute(x, 'fs', [(order[i], order[(i + k) % n]) for i in range(n)])]
    all_gather x3 -> x0, waiting for transfers between devices: 74.8 us -> none  [gather(): return lax.all_gather(x, 'fs', axis=0, tiled=True)]
    ppermute x4 -> x58, waiting for transfers between devices: 9.64 us -> 48.4 us  [the longest x2 14.2 us: scatter_sum(): down = lax.ppermute(far[:, half:], 'fs', self.behind)]
    all_to_all x2 -> x0, waiting for transfers between devices: 34.3 us -> none  [the longest x1 34.3 us: local(): lax.all_to_all(hidden_mine.reshape(n_fs, rows, piece), 'fs', split_axis=0...]
    dot_general x6, matrix products: 33.5 us -> 18.8 us  [contract(): lax.dot_general(left, right, (((left_dim,), (right_dim,)), ((), ())), pre...]
    pallas_call x0 -> x2, Pallas kernels: none -> 14 us  [the longest x1 8.05 us: place_columns(): pl.pallas_call(functools.partial(place_kernel, count), out_shape=jax.Shap...]
    all_to_all x2 -> x0, starting transfers between devices: 10.9 us -> none  [the longest x1 7.31 us: local(): lax.all_to_all(saved_mine, 'fs', split_axis=1, concat_axis=0, tiled=True)]
  transfers between devices with their start and end apart: 11 -> 58, of which waited for: 7 -> 21; matrix products, arithmetic and copies ran while one was open for 20% -> 20% of each run, Pallas kernels for 0% -> 7%
where the time goes in v2:
time: 215 us
  starting transfers between devices  104 us (48%)
  waiting for transfers between devices  48.4 us (23%)
  local copies, waits for them, and re-layouts  22.1 us (10%)
  matrix products  18.8 us (9%)
  Pallas kernels  14 us (7%)
  other arithmetic  6.37 us (3%)
    ppermute x14, starting transfers between devices, shift(): lax.ppermute(x, 'fs', [(order[i], order[(i + k) % n]) for i in range(n)])  30.7 us
    ppermute x6, starting transfers between devices, scatter_sum(): up = lax.ppermute(up, 'fs', self.ahead)  21.6 us
    dot_general x6, matrix products, contract(): lax.dot_general(left, right, (((left_dim,), (right_dim,)), ((), ())), pre...  18.8 us
    ppermute x9, starting transfers between devices, gather(): down = lax.ppermute(down, 'fs', self.behind)  17.2 us
    ppermute x6, starting transfers between devices, scatter_sum(): down = lax.ppermute(down, 'fs', self.behind)  15.5 us
    ppermute x2, waiting for transfers between devices, scatter_sum(): down = lax.ppermute(far[:, half:], 'fs', self.behind)  14.2 us
    unnamed x80, local copies, waits for them, and re-layouts  14.2 us
    ppermute x9, waiting for transfers between devices, gather(): down = lax.ppermute(down, 'fs', self.behind)  12.6 us
  transfers between devices with their start and end apart: 58, of which 21 were waited for; matrix products, arithmetic and copies ran while one was open for 20% of the time, Pallas kernels for 7%

profile of v2, /device:TPU:0, one launch (start us, length us, event | category | flops | bytes accessed | tf_op | source)
XLA Modules:
  0.0 214.9 jit_solution(1644916246074278991)
XLA Ops:
  0.6 3.0 %collective-permute-start.25 = (bf16[128,1024]{1,0:T(8,128)(2,1)}, bf16[128,1024]{1,0:T(8,128)(2,1)}, u32[]{:S(2)}, u32[]{:S(2)}) collective-permute-start(bf16[128,1024]{1,0:T(8,128)(2,1)} %param.13), channel_id=1, source_target_pairs={{4,0},{8,4},{12,8},{14,12},{10,14},{6,10},{2,6},{0,2},{5,1},{9,5},... | collective-permute-start | bytes 786440 | tf_op jit(solution)/shard_map/ppermute | solution.py:68
  7.6 6.0 %pick_columns.1 = bf16[1024,512]{1,0:T(8,128)(2,1)} custom-call(s32[8]{0:T(128)} %get-tuple-element.60.at_ref, bf16[128,8192]{1,0:T(8,128)(2,1)} %x_ref.1), custom_call_target="tpu_custom_call" | custom-call | tf_op jit(solution)/shard_map/pick_columns/pallas_call | solution.py:108
  13.6 2.2 %fusion.14 = (bf16[128,512]{1,0:T(8,128)(2,1)S(1)}, bf16[128,512]{1,0:T(8,128)(2,1)}, bf16[128,512]{1,0:T(8,128)(2,1)}, bf16[128,512]{1,0:T(8,128)(2,1)}, bf16[1...) fusion(bf16[1024,512]{1,0:T(8,128)(2,1)} %pick_columns.1), kind=kLoop, calls=%fused_computation.97 | loop fusion | bytes 2097152 | tf_op jit(solution)/shard_map/slice | solution.py:173
  15.8 1.9 collective-permute-start.34
  17.7 2.6 %collective-permute-start.35 = (bf16[128,512]{1,0:T(8,128)(2,1)}, bf16[128,512]{1,0:T(8,128)(2,1)}, u32[]{:S(2)}, u32[]{:S(2)}) collective-permute-start(bf16[128,512]{1,0:T(8,128)(2,1)} %get-tuple-element.49), channel_id=1, source_target_pairs={{0,6},{4,2},{8,0},{12,4},{14,8},{10,12},{6,14},{2,10},{1,7},{5,3},... | collective-permute-start | bytes 393224 | tf_op jit(solution)/shard_map/ppermute | solution.py:52
  24.5 4.2 %collective-permute-start.37 = (bf16[128,512]{1,0:T(8,128)(2,1)}, bf16[128,512]{1,0:T(8,128)(2,1)S(1)}, u32[]{:S(2)}, u32[]{:S(2)}) collective-permute-start(bf16[128,512]{1,0:T(8,128)(2,1)} %get-tuple-element.47), channel_id=1, source_target_pairs={{0,14},{4,10},{8,6},{12,2},{14,0},{10,4},{6,8},{2,12},{1,15},{5,11... | collective-permute-start | bytes 393224 | tf_op jit(solution)/shard_map/ppermute | solution.py:52
  29.6 5.5 %collective-permute-done.35 = bf16[128,512]{1,0:T(8,128)(2,1)} collective-permute-done((bf16[128,512]{1,0:T(8,128)(2,1)}, bf16[128,512]{1,0:T(8,128)(2,1)}, u32[]{:S(2)}, u32[]{:S(2)}) %collective-permute-start.35) | collective-permute-done | bytes 131104 | tf_op jit(solution)/shard_map/ppermute | solution.py:52
  36.1 2.8 %collective-permute-start.39 = (bf16[128,512]{1,0:T(8,128)(2,1)}, bf16[128,512]{1,0:T(8,128)(2,1)S(1)}, u32[]{:S(2)}, u32[]{:S(2)}) collective-permute-start(bf16[128,512]{1,0:T(8,128)(2,1)} %get-tuple-element.45), channel_id=1, source_target_pairs={{0,8},{4,12},{8,14},{12,10},{14,6},{10,2},{6,0},{2,4},{1,9},{5,13}... | collective-permute-start | bytes 393224 | tf_op jit(solution)/shard_map/ppermute | solution.py:52
  39.8 6.9 %collective-permute-start.40 = (bf16[128,512]{1,0:T(8,128)(2,1)S(1)}, bf16[128,512]{1,0:T(8,128)(2,1)S(1)}, u32[]{:S(2)}, u32[]{:S(2)}) collective-permute-start(bf16[128,512]{1,0:T(8,128)(2,1)S(1)} %get-tuple-element.44), channel_id=1, source_target_pairs={{0,4},{4,8},{8,12},{12,14},{14,10},{10,6},{6,2},{2,0},{1,5},{5,9},... | collective-permute-start | bytes 393224 | tf_op jit(solution)/shard_map/ppermute | solution.py:52
  46.7 2.2 %collective-permute-done.38 = bf16[128,512]{1,0:T(8,128)(2,1)S(1)} collective-permute-done((bf16[128,512]{1,0:T(8,128)(2,1)}, bf16[128,512]{1,0:T(8,128)(2,1)S(1)}, u32[]{:S(2)}, u32[]{:S(2)}) %collective-permute-start.38) | collective-permute-done | bytes 131104 | tf_op jit(solution)/shard_map/ppermute | solution.py:52
  49.0 2.1 collective-permute-start.53
  53.2 2.7 %collective-permute-start.26 = (bf16[128,1024]{1,0:T(8,128)(2,1)}, bf16[128,1024]{1,0:T(8,128)(2,1)S(1)}, u32[]{:S(2)}, u32[]{:S(2)}) collective-permute-start(bf16[128,1024]{1,0:T(8,128)(2,1)} %collective-permute-done.25), channel_id=1, source_target_pairs={{4,0},{8,4},{12,8},{14,12},{10,14},{6,10},{2,6},{0,2},{5,1},{9,5},... | collective-permute-start | bytes 786440 | tf_op jit(solution)/shard_map/ppermute | solution.py:68
  55.9 2.5 %collective-permute-done.50 = bf16[128,1024]{1,0:T(8,128)(2,1)S(1)} collective-permute-done((bf16[128,1024]{1,0:T(8,128)(2,1)}, bf16[128,1024]{1,0:T(8,128)(2,1)S(1)}, u32[]{:S(2)}, u32[]{:S(2)}) %collective-permute-start.50) | collective-permute-done | bytes 262176 | tf_op jit(solution)/shard_map/ppermute | solution.py:68
  60.0 2.0 collective-permute-start.51
  62.0 1.9 collective-permute-done
  65.3 2.0 collective-permute-start.1
  67.3 2.2 %collective-permute-done.26 = bf16[128,1024]{1,0:T(8,128)(2,1)S(1)} collective-permute-done((bf16[128,1024]{1,0:T(8,128)(2,1)}, bf16[128,1024]{1,0:T(8,128)(2,1)S(1)}, u32[]{:S(2)}, u32[]{:S(2)}) %collective-permute-start.26) | collective-permute-done | bytes 262176 | tf_op jit(solution)/shard_map/ppermute | solution.py:68
  70.9 2.0 collective-permute-start.27
  76.5 2.0 collective-permute-start.52
  82.2 2.0 collective-permute-start.2
  84.2 1.8 collective-permute-done.27
  91.0 3.5 %collective-permute-start.32 = (bf16[64,1024]{1,0:T(8,128)(2,1)S(1)}, bf16[64,1024]{1,0:T(8,128)(2,1)S(1)}, u32[]{:S(2)}, u32[]{:S(2)}) collective-permute-start(bf16[64,1024]{1,0:T(8,128)(2,1)S(1)} %slice.250), channel_id=1, source_target_pairs={{4,0},{8,4},{12,8},{14,12},{10,14},{6,10},{2,6},{0,2},{5,1},{9,5},... | collective-permute-start | bytes 393224 | tf_op jit(solution)/shard_map/ppermute | solution.py:71
  96.5 3.5 %collective-permute-start.57 = (bf16[64,1024]{1,0:T(8,128)(2,1)S(1)}, bf16[64,1024]{1,0:T(8,128)(2,1)S(1)}, u32[]{:S(2)}, u32[]{:S(2)}) collective-permute-start(bf16[64,1024]{1,0:T(8,128)(2,1)S(1)} %slice.271), channel_id=1, source_target_pairs={{4,0},{8,4},{12,8},{14,12},{10,14},{6,10},{2,6},{0,2},{5,1},{9,5},... | collective-permute-start | bytes 393224 | tf_op jit(solution)/shard_map/ppermute | solution.py:71
  100.1 2.3 %collective-permute-start.7 = (bf16[64,1024]{1,0:T(8,128)(2,1)S(1)}, bf16[64,1024]{1,0:T(8,128)(2,1)S(1)}, u32[]{:S(2)}, u32[]{:S(2)}) collective-permute-start(bf16[64,1024]{1,0:T(8,128)(2,1)S(1)} %slice.229), channel_id=1, source_target_pairs={{4,0},{8,4},{12,8},{14,12},{10,14},{6,10},{2,6},{0,2},{5,1},{9,5},... | collective-permute-start | bytes 393224 | tf_op jit(solution)/shard_map/ppermute | solution.py:71
  103.5 2.4 %convolution_convert_fusion.1 = bf16[1024,1024]{1,0:T(8,128)(2,1)S(1)} fusion(bf16[1024,1024]{1,0:T(8,128)(2,1)S(1)} %constant_dynamic-update-slice_fusion.17, bf16[1024,1024]{1,0:T(8,128)(2,1)S(1)} %copy-done.20), kind=kOutput, calls=%fused_computation.15 | convolution fusion | flops 2148532224 | bytes 6291456 | tf_op jit(solution)/shard_map/dot_general | solution.py:12
  106.1 2.3 %convolution_convert_fusion.2 = bf16[1024,1024]{1,0:T(8,128)(2,1)S(1)} fusion(bf16[1024,1024]{1,0:T(8,128)(2,1)S(1)} %constant_dynamic-update-slice_fusion, bf16[1024,1024]{1,0:T(8,128)(2,1)S(1)} %copy-done), kind=kOutput, calls=%fused_computation.16 | convolution fusion | flops 2148532224 | bytes 6291456 | tf_op jit(solution)/shard_map/dot_general | solution.py:12
  109.5 1.9 copy-done.18
  111.4 4.5 %fusion.4 = f32[1024,1024]{1,0:T(8,128)} fusion(f32[1024,1024]{1,0:T(8,128)S(1)} %copy-done.18, bf16[1024,1024]{1,0:T(8,128)(2,1)S(1)} %constant_dynamic-update-slice_fusion.17, bf16[1024,512]{1,0:T(8,128)(2,1)S(1)} %get-tuple-element.26, bf16[1024,512]{1,0:T(8,128)(2,1)S(1)} %get-tuple-element.25), kind=kOutput, calls=%fused_computation.11 | convolution fusion | flops 2155872256 | bytes 12582912 | tf_op jit(solution)/shard_map/dot_general | solution.py:12
  115.8 2.5 %convolution_convert_fusion = bf16[1024,1024]{0,1:T(8,128)(2,1)S(1)} fusion(bf16[1024,1024]{1,0:T(8,128)(2,1)S(1)} %copy-done, bf16[1024,1024]{1,0:T(8,128)(2,1)S(1)} %collective-permute-done.33, bf16[1024,1024]{1,0:T(8,128)(2,1)S(1)} %convolution_convert_fusion.1, bf16[1024,512]{1,0:T(8,128)(2,1)S(1)} %get-tuple-element.26, ...), kind=kOutput, calls=%fused_computation.14 | convolution fusion | flops 2160066560 | bytes 10485760 | tf_op jit(solution)/shard_map/dot_general | solution.py:12
  121.9 2.4 %fusion.5 = bf16[1024,1024]{0,1:T(8,128)(2,1)S(1)} fusion(bf16[1024,1024]{1,0:T(8,128)(2,1)S(1)} %copy-done.20, bf16[1024,1024]{1,0:T(8,128)(2,1)S(1)} %add_convert_fusion), kind=kOutput, calls=%fused_computation.13 | convolution fusion | flops 2152726528 | bytes 6291456 | tf_op jit(solution)/shard_map/dot_general | solution.py:12
  125.2 1.7 collective-permute-start.17
  128.6 2.2 %collective-permute-start.19 = (bf16[128,512]{1,0:T(8,128)(2,1)S(1)}, bf16[128,512]{1,0:T(8,128)(2,1)S(1)}, u32[]{:S(2)}, u32[]{:S(2)}) collective-permute-start(bf16[128,512]{1,0:T(8,128)(2,1)S(1)} %get-tuple-element.31), channel_id=1, source_target_pairs={{0,10},{4,6},{8,2},{12,0},{14,4},{10,8},{6,12},{2,14},{1,11},{5,7}... | collective-permute-start | bytes 393224 | tf_op jit(solution)/shard_map/ppermute | solution.py:52
  130.9 2.0 collective-permute-start.9
  133.0 14.2 %collective-permute-done.13 = bf16[128,512]{0,1:T(8,128)(2,1)S(1)} collective-permute-done((bf16[128,512]{0,1:T(8,128)(2,1)S(1)}, bf16[128,512]{0,1:T(8,128)(2,1)S(1)}, u32[]{:S(2)}, u32[]{:S(2)}) %collective-permute-start.13) | collective-permute-done | bytes 131104 | tf_op jit(solution)/shard_map/ppermute | solution.py:84
  147.3 2.8 %collective-permute-start.20 = (bf16[128,512]{1,0:T(8,128)(2,1)S(1)}, bf16[128,512]{1,0:T(8,128)(2,1)S(1)}, u32[]{:S(2)}, u32[]{:S(2)}) collective-permute-start(bf16[128,512]{1,0:T(8,128)(2,1)S(1)} %get-tuple-element.30), channel_id=1, source_target_pairs={{0,14},{4,10},{8,6},{12,2},{14,0},{10,4},{6,8},{2,12},{1,15},{5,11... | collective-permute-start | bytes 393224 | tf_op jit(solution)/shard_map/ppermute | solution.py:52
  150.2 1.8 collective-permute-start.22
  154.4 2.0 collective-permute-done.20.refs_4_
  156.4 7.3 %collective-permute-start.43 = (bf16[128,1024]{0,1:T(8,128)(2,1)S(1)}, bf16[128,1024]{0,1:T(8,128)(2,1)S(1)}, u32[]{:S(2)}, u32[]{:S(2)}) collective-permute-start(bf16[128,1024]{0,1:T(8,128)(2,1)S(1)} %pad_maximum_fusion.4), channel_id=1, source_target_pairs={{0,4},{4,8},{8,12},{12,14},{14,10},{10,6},{6,2},{2,0},{1,5},{5,9},... | collective-permute-start | bytes 786440 | tf_op jit(solution)/shard_map/ppermute | solution.py:94
  163.8 2.3 %collective-permute-done.21.refs_5_ = bf16[128,512]{1,0:T(8,128)(2,1)S(1)} collective-permute-done((bf16[128,512]{1,0:T(8,128)(2,1)S(1)}, bf16[128,512]{1,0:T(8,128)(2,1)S(1)}, u32[]{:S(2)}, u32[]{:S(2)}) %collective-permute-start.21) | collective-permute-done | bytes 131104 | tf_op jit(solution)/shard_map/ppermute | solution.py:52
  166.2 3.2 %collective-permute-start.14 = (bf16[128,1024]{0,1:T(8,128)(2,1)S(1)}, bf16[128,1024]{0,1:T(8,128)(2,1)S(1)}, u32[]{:S(2)}, u32[]{:S(2)}) collective-permute-start(bf16[128,1024]{0,1:T(8,128)(2,1)S(1)} %pad_maximum_fusion.3), channel_id=1, source_target_pairs={{4,0},{8,4},{12,8},{14,12},{10,14},{6,10},{2,6},{0,2},{5,1},{9,5},... | collective-permute-start | bytes 786440 | tf_op jit(solution)/shard_map/ppermute | solution.py:95
  170.5 6.0 %collective-permute-start.44 = (bf16[128,1024]{0,1:T(8,128)(2,1)S(1)}, bf16[128,1024]{0,1:T(8,128)(2,1)S(1)}, u32[]{:S(2)}, u32[]{:S(2)}) collective-permute-start(bf16[128,1024]{0,1:T(8,128)(2,1)S(1)} %add_convert_fusion.5), channel_id=1, source_target_pairs={{0,4},{4,8},{8,12},{12,14},{14,10},{10,6},{6,2},{2,0},{1,5},{5,9},... | collective-permute-start | bytes 786440 | tf_op jit(solution)/shard_map/ppermute | solution.py:94
  176.6 5.5 %collective-permute-start.11 = (bf16[128,1024]{0,1:T(8,128)(2,1)S(1)}, bf16[128,1024]{0,1:T(8,128)(2,1)S(1)}, u32[]{:S(2)}, u32[]{:S(2)}) collective-permute-start(bf16[128,1024]{0,1:T(8,128)(2,1)S(1)} %add_convert_fusion.10), channel_id=1, source_target_pairs={{0,4},{4,8},{8,12},{12,14},{14,10},{10,6},{6,2},{2,0},{1,5},{5,9},... | collective-permute-start | bytes 786440 | tf_op jit(solution)/shard_map/ppermute | solution.py:94
  182.4 4.1 %collective-permute-start.48 = (bf16[128,1024]{0,1:T(8,128)(2,1)S(1)}, bf16[128,1024]{0,1:T(8,128)(2,1)S(1)}, u32[]{:S(2)}, u32[]{:S(2)}) collective-permute-start(bf16[128,1024]{0,1:T(8,128)(2,1)S(1)} %get-tuple-element.18), channel_id=1, source_target_pairs={{4,0},{8,4},{12,8},{14,12},{10,14},{6,10},{2,6},{0,2},{5,1},{9,5},... | collective-permute-start | bytes 786440 | tf_op jit(solution)/shard_map/ppermute | solution.py:95
  187.4 4.6 %collective-permute-start.15 = (bf16[128,1024]{0,1:T(8,128)(2,1)S(1)}, bf16[128,1024]{0,1:T(8,128)(2,1)S(1)}, u32[]{:S(2)}, u32[]{:S(2)}) collective-permute-start(bf16[128,1024]{0,1:T(8,128)(2,1)S(1)} %get-tuple-element.37), channel_id=1, source_target_pairs={{4,0},{8,4},{12,8},{14,12},{10,14},{6,10},{2,6},{0,2},{5,1},{9,5},... | collective-permute-start | bytes 786440 | tf_op jit(solution)/shard_map/ppermute | solution.py:95
  192.1 4.7 %convolution_add_fusion = f32[1024,1024]{1,0:T(8,128)} fusion(f32[1024,1024]{1,0:T(8,128)S(1)} %copy-done.19, bf16[1024,1024]{1,0:T(8,128)(2,1)S(1)} %constant_dynamic-update-slice_fusion.33, bf16[1024,1024]{1,0:T(8,128)(2,1)S(1)} %collective-permute-done.33, bf16[1024,1024]{1,0:T(8,128)(2,1)S(1)} %convolution_convert_fusion.1, ...), kind=kOutput, calls=%fused_computation.12 | convolution fusion | flops 2160066560 | bytes 16777216 | tf_op jit(solution)/shard_map/dot_general | solution.py:12
  197.1 2.5 %collective-permute-start.12 = (bf16[128,1024]{0,1:T(8,128)(2,1)S(1)}, bf16[128,1024]{0,1:T(8,128)(2,1)S(1)}, u32[]{:S(2)}, u32[]{:S(2)}) collective-permute-start(bf16[128,1024]{0,1:T(8,128)(2,1)S(1)} %get-tuple-element.36), channel_id=1, source_target_pairs={{0,4},{4,8},{8,12},{12,14},{14,10},{10,6},{6,2},{2,0},{1,5},{5,9},... | collective-permute-start | bytes 786440 | tf_op jit(solution)/shard_map/ppermute | solution.py:94
  199.9 1.9 collective-permute-start.16
  202.8 8.0 %place_columns.1 = bf16[128,8192]{1,0:T(8,128)(2,1)} custom-call(s32[16]{0:T(128)} %pad_add_fusion.at_ref, bf16[128,512]{1,0:T(8,128)(2,1)} %get-tuple-element.35.refs_0_, bf16[128,512]{1,0:T(8,128)(2,1)} %copy-done.4, bf16[128,512]{1,0:T(8,128)(2,1)} %copy-done.5, bf16[128,512]{1,0:T(8,128)(2,1)} %copy-done.6, bf16[128,512]{1,0:T(8,128)(2,1)} %copy-done.7, ...), custom_call_target="tpu_custom_call" | custom-call | tf_op jit(solution)/shard_map/place_columns/pallas_call | solution.py:133
  (194 shorter events, 50.4 us)
Async XLA Ops:
  0.6 51.8 %collective-permute-start.25 = (bf16[128,1024]{1,0:T(8,128)(2,1)}, bf16[128,1024]{1,0:T(8,128)(2,1)}, u32[]{:S(2)}, u32[]{:S(2)}) collective-permute-start(bf16[128,1024]{1,0:T(8,128)(2,1)} %param.13), channel_id=1, source_target_pairs={{4,0},{8,4},{12,8},{14,12},{10,14},{6,10},{2,6},{0,2},{5,1},{9,5},... | collective-permute-start | bytes 786440 | tf_op jit(solution)/shard_map/ppermute | solution.py:68
  3.7 49.5 %collective-permute-start.28 = (bf16[128,1024]{1,0:T(8,128)(2,1)}, bf16[128,1024]{1,0:T(8,128)(2,1)}, u32[]{:S(2)}, u32[]{:S(2)}) collective-permute-start(bf16[128,1024]{1,0:T(8,128)(2,1)} %param.13), channel_id=1, source_target_pairs={{0,4},{4,8},{8,12},{12,14},{14,10},{10,6},{6,2},{2,0},{1,5},{5,9},... | collective-permute-start | bytes 786440 | tf_op jit(solution)/shard_map/ppermute | solution.py:67
  17.7 17.4 %collective-permute-start.35 = (bf16[128,512]{1,0:T(8,128)(2,1)}, bf16[128,512]{1,0:T(8,128)(2,1)}, u32[]{:S(2)}, u32[]{:S(2)}) collective-permute-start(bf16[128,512]{1,0:T(8,128)(2,1)} %get-tuple-element.49), channel_id=1, source_target_pairs={{0,6},{4,2},{8,0},{12,4},{14,8},{10,12},{6,14},{2,10},{1,7},{5,3},... | collective-permute-start | bytes 393224 | tf_op jit(solution)/shard_map/ppermute | solution.py:52
  20.3 15.7 %collective-permute-start.36 = (bf16[128,512]{1,0:T(8,128)(2,1)}, bf16[128,512]{1,0:T(8,128)(2,1)}, u32[]{:S(2)}, u32[]{:S(2)}) collective-permute-start(bf16[128,512]{1,0:T(8,128)(2,1)} %get-tuple-element.48), channel_id=1, source_target_pairs={{0,10},{4,6},{8,2},{12,0},{14,4},{10,8},{6,12},{2,14},{1,11},{5,7}... | collective-permute-start | bytes 393224 | tf_op jit(solution)/shard_map/ppermute | solution.py:52
  24.5 15.2 %collective-permute-start.37 = (bf16[128,512]{1,0:T(8,128)(2,1)}, bf16[128,512]{1,0:T(8,128)(2,1)S(1)}, u32[]{:S(2)}, u32[]{:S(2)}) collective-permute-start(bf16[128,512]{1,0:T(8,128)(2,1)} %get-tuple-element.47), channel_id=1, source_target_pairs={{0,14},{4,10},{8,6},{12,2},{14,0},{10,4},{6,8},{2,12},{1,15},{5,11... | collective-permute-start | bytes 393224 | tf_op jit(solution)/shard_map/ppermute | solution.py:52
  35.1 13.8 %collective-permute-start.38 = (bf16[128,512]{1,0:T(8,128)(2,1)}, bf16[128,512]{1,0:T(8,128)(2,1)S(1)}, u32[]{:S(2)}, u32[]{:S(2)}) collective-permute-start(bf16[128,512]{1,0:T(8,128)(2,1)} %get-tuple-element.46), channel_id=1, source_target_pairs={{0,12},{4,14},{8,10},{12,6},{14,2},{10,0},{6,4},{2,8},{1,13},{5,15... | collective-permute-start | bytes 393224 | tf_op jit(solution)/shard_map/ppermute | solution.py:52
  36.1 12.9 %collective-permute-start.39 = (bf16[128,512]{1,0:T(8,128)(2,1)}, bf16[128,512]{1,0:T(8,128)(2,1)S(1)}, u32[]{:S(2)}, u32[]{:S(2)}) collective-permute-start(bf16[128,512]{1,0:T(8,128)(2,1)} %get-tuple-element.45), channel_id=1, source_target_pairs={{0,8},{4,12},{8,14},{12,10},{14,6},{10,2},{6,0},{2,4},{1,9},{5,13}... | collective-permute-start | bytes 393224 | tf_op jit(solution)/shard_map/ppermute | solution.py:52
  39.8 11.3 %collective-permute-start.40 = (bf16[128,512]{1,0:T(8,128)(2,1)S(1)}, bf16[128,512]{1,0:T(8,128)(2,1)S(1)}, u32[]{:S(2)}, u32[]{:S(2)}) collective-permute-start(bf16[128,512]{1,0:T(8,128)(2,1)S(1)} %get-tuple-element.44), channel_id=1, source_target_pairs={{0,4},{4,8},{8,12},{12,14},{14,10},{10,6},{6,2},{2,0},{1,5},{5,9},... | collective-permute-start | bytes 393224 | tf_op jit(solution)/shard_map/ppermute | solution.py:52
  49.0 11.0 %collective-permute-start.53 = (bf16[128,1024]{1,0:T(8,128)(2,1)}, bf16[128,1024]{1,0:T(8,128)(2,1)S(1)}, u32[]{:S(2)}, u32[]{:S(2)}) collective-permute-start(bf16[128,1024]{1,0:T(8,128)(2,1)} %param.11), channel_id=1, source_target_pairs={{0,4},{4,8},{8,12},{12,14},{14,10},{10,6},{6,2},{2,0},{1,5},{5,9},... | collective-permute-start | bytes 786440 | tf_op jit(solution)/shard_map/ppermute | solution.py:67
  51.1 12.9 %collective-permute-start = (bf16[128,1024]{1,0:T(8,128)(2,1)}, bf16[128,1024]{1,0:T(8,128)(2,1)S(1)}, u32[]{:S(2)}, u32[]{:S(2)}) collective-permute-start(bf16[128,1024]{1,0:T(8,128)(2,1)} %param.10), channel_id=1, source_target_pairs={{4,0},{8,4},{12,8},{14,12},{10,14},{6,10},{2,6},{0,2},{5,1},{9,5},... | collective-permute-start | bytes 786440 | tf_op jit(solution)/shard_map/ppermute | solution.py:68
  52.4 12.9 %collective-permute-start.3 = (bf16[128,1024]{1,0:T(8,128)(2,1)}, bf16[128,1024]{1,0:T(8,128)(2,1)S(1)}, u32[]{:S(2)}, u32[]{:S(2)}) collective-permute-start(bf16[128,1024]{1,0:T(8,128)(2,1)} %param.10), channel_id=1, source_target_pairs={{0,4},{4,8},{8,12},{12,14},{14,10},{10,6},{6,2},{2,0},{1,5},{5,9},... | collective-permute-start | bytes 786440 | tf_op jit(solution)/shard_map/ppermute | solution.py:67
  53.2 16.4 %collective-permute-start.26 = (bf16[128,1024]{1,0:T(8,128)(2,1)}, bf16[128,1024]{1,0:T(8,128)(2,1)S(1)}, u32[]{:S(2)}, u32[]{:S(2)}) collective-permute-start(bf16[128,1024]{1,0:T(8,128)(2,1)} %collective-permute-done.25), channel_id=1, source_target_pairs={{4,0},{8,4},{12,8},{14,12},{10,14},{6,10},{2,6},{0,2},{5,1},{9,5},... | collective-permute-start | bytes 786440 | tf_op jit(solution)/shard_map/ppermute | solution.py:68
  58.3 12.6 %collective-permute-start.29 = (bf16[128,1024]{1,0:T(8,128)(2,1)}, bf16[128,1024]{1,0:T(8,128)(2,1)S(1)}, u32[]{:S(2)}, u32[]{:S(2)}) collective-permute-start(bf16[128,1024]{1,0:T(8,128)(2,1)} %collective-permute-done.28), channel_id=1, source_target_pairs={{0,4},{4,8},{8,12},{12,14},{14,10},{10,6},{6,2},{2,0},{1,5},{5,9},... | collective-permute-start | bytes 786440 | tf_op jit(solution)/shard_map/ppermute | solution.py:67
  60.0 15.2 %collective-permute-start.51 = (bf16[128,1024]{1,0:T(8,128)(2,1)S(1)}, bf16[128,1024]{1,0:T(8,128)(2,1)S(1)}, u32[]{:S(2)}, u32[]{:S(2)}) collective-permute-start(bf16[128,1024]{1,0:T(8,128)(2,1)S(1)} %collective-permute-done.50), channel_id=1, source_target_pairs={{4,0},{8,4},{12,8},{14,12},{10,14},{6,10},{2,6},{0,2},{5,1},{9,5},... | collective-permute-start | bytes 786440 | tf_op jit(solution)/shard_map/ppermute | solution.py:68
  64.0 12.6 %collective-permute-start.54 = (bf16[128,1024]{1,0:T(8,128)(2,1)S(1)}, bf16[128,1024]{1,0:T(8,128)(2,1)S(1)}, u32[]{:S(2)}, u32[]{:S(2)}) collective-permute-start(bf16[128,1024]{1,0:T(8,128)(2,1)S(1)} %collective-permute-done.53), channel_id=1, source_target_pairs={{0,4},{4,8},{8,12},{12,14},{14,10},{10,6},{6,2},{2,0},{1,5},{5,9},... | collective-permute-start | bytes 786440 | tf_op jit(solution)/shard_map/ppermute | solution.py:67
  65.3 15.5 %collective-permute-start.1 = (bf16[128,1024]{1,0:T(8,128)(2,1)S(1)}, bf16[128,1024]{1,0:T(8,128)(2,1)S(1)}, u32[]{:S(2)}, u32[]{:S(2)}) collective-permute-start(bf16[128,1024]{1,0:T(8,128)(2,1)S(1)} %collective-permute-done), channel_id=1, source_target_pairs={{4,0},{8,4},{12,8},{14,12},{10,14},{6,10},{2,6},{0,2},{5,1},{9,5},... | collective-permute-start | bytes 786440 | tf_op jit(solution)/shard_map/ppermute | solution.py:68
  69.6 12.6 %collective-permute-start.4 = (bf16[128,1024]{1,0:T(8,128)(2,1)S(1)}, bf16[128,1024]{1,0:T(8,128)(2,1)S(1)}, u32[]{:S(2)}, u32[]{:S(2)}) collective-permute-start(bf16[128,1024]{1,0:T(8,128)(2,1)S(1)} %collective-permute-done.3), channel_id=1, source_target_pairs={{0,4},{4,8},{8,12},{12,14},{14,10},{10,6},{6,2},{2,0},{1,5},{5,9},... | collective-permute-start | bytes 786440 | tf_op jit(solution)/shard_map/ppermute | solution.py:67
  70.9 15.1 %collective-permute-start.27 = (bf16[128,1024]{1,0:T(8,128)(2,1)S(1)}, bf16[128,1024]{1,0:T(8,128)(2,1)S(1)}, u32[]{:S(2)}, u32[]{:S(2)}) collective-permute-start(bf16[128,1024]{1,0:T(8,128)(2,1)S(1)} %collective-permute-done.26), channel_id=1, source_target_pairs={{4,0},{8,4},{12,8},{14,12},{10,14},{6,10},{2,6},{0,2},{5,1},{9,5},... | collective-permute-start | bytes 786440 | tf_op jit(solution)/shard_map/ppermute | solution.py:68
  75.2 12.6 %collective-permute-start.30 = (bf16[128,1024]{1,0:T(8,128)(2,1)S(1)}, bf16[128,1024]{1,0:T(8,128)(2,1)S(1)}, u32[]{:S(2)}, u32[]{:S(2)}) collective-permute-start(bf16[128,1024]{1,0:T(8,128)(2,1)S(1)} %collective-permute-done.29), channel_id=1, source_target_pairs={{0,4},{4,8},{8,12},{12,14},{14,10},{10,6},{6,2},{2,0},{1,5},{5,9},... | collective-permute-start | bytes 786440 | tf_op jit(solution)/shard_map/ppermute | solution.py:67
  76.5 12.3 %collective-permute-start.52 = (bf16[128,1024]{1,0:T(8,128)(2,1)S(1)}, bf16[128,1024]{1,0:T(8,128)(2,1)S(1)}, u32[]{:S(2)}, u32[]{:S(2)}) collective-permute-start(bf16[128,1024]{1,0:T(8,128)(2,1)S(1)} %collective-permute-done.51), channel_id=1, source_target_pairs={{4,0},{8,4},{12,8},{14,12},{10,14},{6,10},{2,6},{0,2},{5,1},{9,5},... | collective-permute-start | bytes 786440 | tf_op jit(solution)/shard_map/ppermute | solution.py:68
  82.2 12.4 %collective-permute-start.2 = (bf16[128,1024]{1,0:T(8,128)(2,1)S(1)}, bf16[128,1024]{1,0:T(8,128)(2,1)S(1)}, u32[]{:S(2)}, u32[]{:S(2)}) collective-permute-start(bf16[128,1024]{1,0:T(8,128)(2,1)S(1)} %collective-permute-done.1), channel_id=1, source_target_pairs={{4,0},{8,4},{12,8},{14,12},{10,14},{6,10},{2,6},{0,2},{5,1},{9,5},... | collective-permute-start | bytes 786440 | tf_op jit(solution)/shard_map/ppermute | solution.py:68
  87.8 21.4 %collective-permute-start.41 = (bf16[1024,512]{1,0:T(8,128)(2,1)S(1)}, bf16[1024,512]{1,0:T(8,128)(2,1)S(1)}, u32[]{:S(2)}, u32[]{:S(2)}) collective-permute-start(bf16[1024,512]{1,0:T(8,128)(2,1)S(1)} %constant_dynamic-update-slice_fusion.26), channel_id=1, source_target_pairs={{0,1},{1,0},{2,3},{3,2},{4,5},{5,4},{6,7},{7,6},{8,9},{9,8},{10,11... | collective-permute-start | bytes 3145736 | tf_op jit(solution)/shard_map/ppermute | solution.py:147
  88.9 11.1 %collective-permute-start.31 = (bf16[64,1024]{1,0:T(8,128)(2,1)S(1)}, bf16[64,1024]{1,0:T(8,128)(2,1)S(1)}, u32[]{:S(2)}, u32[]{:S(2)}) collective-permute-start(bf16[64,1024]{1,0:T(8,128)(2,1)S(1)} %slice.249), channel_id=1, source_target_pairs={{0,4},{4,8},{8,12},{12,14},{14,10},{10,6},{6,2},{2,0},{1,5},{5,9},... | collective-permute-start | bytes 393224 | tf_op jit(solution)/shard_map/ppermute | solution.py:71
  94.6 14.5 %collective-permute-start.56 = (bf16[64,1024]{1,0:T(8,128)(2,1)S(1)}, bf16[64,1024]{1,0:T(8,128)(2,1)S(1)}, u32[]{:S(2)}, u32[]{:S(2)}) collective-permute-start(bf16[64,1024]{1,0:T(8,128)(2,1)S(1)} %slice.270), channel_id=1, source_target_pairs={{0,4},{4,8},{8,12},{12,14},{14,10},{10,6},{6,2},{2,0},{1,5},{5,9},... | collective-permute-start | bytes 393224 | tf_op jit(solution)/shard_map/ppermute | solution.py:71
  96.5 12.6 %collective-permute-start.57 = (bf16[64,1024]{1,0:T(8,128)(2,1)S(1)}, bf16[64,1024]{1,0:T(8,128)(2,1)S(1)}, u32[]{:S(2)}, u32[]{:S(2)}) collective-permute-start(bf16[64,1024]{1,0:T(8,128)(2,1)S(1)} %slice.271), channel_id=1, source_target_pairs={{4,0},{8,4},{12,8},{14,12},{10,14},{6,10},{2,6},{0,2},{5,1},{9,5},... | collective-permute-start | bytes 393224 | tf_op jit(solution)/shard_map/ppermute | solution.py:71
  108.5 12.3 %collective-permute-start.8 = (bf16[1024,1024]{1,0:T(8,128)(2,1)S(1)}, bf16[1024,1024]{1,0:T(8,128)(2,1)S(1)}, u32[]{:S(2)}, u32[]{:S(2)}) collective-permute-start(bf16[1024,1024]{1,0:T(8,128)(2,1)S(1)} %convolution_convert_fusion.2), channel_id=1, source_target_pairs={{0,1},{1,0},{2,3},{3,2},{4,5},{5,4},{6,7},{7,6},{8,9},{9,8},{10,11... | collective-permute-start | bytes 6291464 | tf_op jit(solution)/shard_map/ppermute | solution.py:147
  118.5 12.4 %collective-permute-start.42 = (bf16[128,512]{0,1:T(8,128)(2,1)S(1)}, bf16[128,512]{0,1:T(8,128)(2,1)S(1)}, u32[]{:S(2)}, u32[]{:S(2)}) collective-permute-start(bf16[128,512]{0,1:T(8,128)(2,1)S(1)} %get-tuple-element.21), channel_id=1, source_target_pairs={{0,4},{4,8},{8,12},{12,14},{14,10},{10,6},{6,2},{2,0},{1,5},{5,9},... | collective-permute-start | bytes 393224 | tf_op jit(solution)/shard_map/ppermute | solution.py:83
  120.0 11.0 %collective-permute-start.46 = (bf16[128,512]{0,1:T(8,128)(2,1)S(1)}, bf16[128,512]{0,1:T(8,128)(2,1)S(1)}, u32[]{:S(2)}, u32[]{:S(2)}) collective-permute-start(bf16[128,512]{0,1:T(8,128)(2,1)S(1)} %get-tuple-element.22), channel_id=1, source_target_pairs={{4,0},{8,4},{12,8},{14,12},{10,14},{6,10},{2,6},{0,2},{5,1},{9,5},... | collective-permute-start | bytes 393224 | tf_op jit(solution)/shard_map/ppermute | solution.py:84
  125.2 24.9 %collective-permute-start.17 = (bf16[128,512]{1,0:T(8,128)(2,1)S(1)}, bf16[128,512]{1,0:T(8,128)(2,1)S(1)}, u32[]{:S(2)}, u32[]{:S(2)}) collective-permute-start(bf16[128,512]{1,0:T(8,128)(2,1)S(1)} %get-tuple-element.33), channel_id=1, source_target_pairs={{0,2},{4,0},{8,4},{12,8},{14,12},{10,14},{6,10},{2,6},{1,3},{5,1},... | collective-permute-start | bytes 393224 | tf_op jit(solution)/shard_map/ppermute | solution.py:52
  127.0 25.0 %collective-permute-start.18 = (bf16[128,512]{1,0:T(8,128)(2,1)S(1)}, bf16[128,512]{1,0:T(8,128)(2,1)S(1)}, u32[]{:S(2)}, u32[]{:S(2)}) collective-permute-start(bf16[128,512]{1,0:T(8,128)(2,1)S(1)} %get-tuple-element.32), channel_id=1, source_target_pairs={{0,6},{4,2},{8,0},{12,4},{14,8},{10,12},{6,14},{2,10},{1,7},{5,3},... | collective-permute-start | bytes 393224 | tf_op jit(solution)/shard_map/ppermute | solution.py:52
  128.6 24.2 %collective-permute-start.19 = (bf16[128,512]{1,0:T(8,128)(2,1)S(1)}, bf16[128,512]{1,0:T(8,128)(2,1)S(1)}, u32[]{:S(2)}, u32[]{:S(2)}) collective-permute-start(bf16[128,512]{1,0:T(8,128)(2,1)S(1)} %get-tuple-element.31), channel_id=1, source_target_pairs={{0,10},{4,6},{8,2},{12,0},{14,4},{10,8},{6,12},{2,14},{1,11},{5,7}... | collective-permute-start | bytes 393224 | tf_op jit(solution)/shard_map/ppermute | solution.py:52
  130.9 16.4 %collective-permute-start.13 = (bf16[128,512]{0,1:T(8,128)(2,1)S(1)}, bf16[128,512]{0,1:T(8,128)(2,1)S(1)}, u32[]{:S(2)}, u32[]{:S(2)}) collective-permute-start(bf16[128,512]{0,1:T(8,128)(2,1)S(1)} %get-tuple-element.41), channel_id=1, source_target_pairs={{4,0},{8,4},{12,8},{14,12},{10,14},{6,10},{2,6},{0,2},{5,1},{9,5},... | collective-permute-start | bytes 393224 | tf_op jit(solution)/shard_map/ppermute | solution.py:84
  130.9 19.1 %collective-permute-start.9 = (bf16[128,512]{0,1:T(8,128)(2,1)S(1)}, bf16[128,512]{0,1:T(8,128)(2,1)S(1)}, u32[]{:S(2)}, u32[]{:S(2)}) collective-permute-start(bf16[128,512]{0,1:T(8,128)(2,1)S(1)} %get-tuple-element.40), channel_id=1, source_target_pairs={{0,4},{4,8},{8,12},{12,14},{14,10},{10,6},{6,2},{2,0},{1,5},{5,9},... | collective-permute-start | bytes 393224 | tf_op jit(solution)/shard_map/ppermute | solution.py:83
  150.1 16.0 %collective-permute-start.21 = (bf16[128,512]{1,0:T(8,128)(2,1)S(1)}, bf16[128,512]{1,0:T(8,128)(2,1)S(1)}, u32[]{:S(2)}, u32[]{:S(2)}) collective-permute-start(bf16[128,512]{1,0:T(8,128)(2,1)S(1)} %get-tuple-element.29), channel_id=1, source_target_pairs={{0,12},{4,14},{8,10},{12,6},{14,2},{10,0},{6,4},{2,8},{1,13},{5,15... | collective-permute-start | bytes 393224 | tf_op jit(solution)/shard_map/ppermute | solution.py:52
  150.2 16.0 %collective-permute-start.22 = (bf16[128,512]{1,0:T(8,128)(2,1)S(1)}, bf16[128,512]{1,0:T(8,128)(2,1)S(1)}, u32[]{:S(2)}, u32[]{:S(2)}) collective-permute-start(bf16[128,512]{1,0:T(8,128)(2,1)S(1)} %get-tuple-element.28), channel_id=1, source_target_pairs={{0,8},{4,12},{8,14},{12,10},{14,6},{10,2},{6,0},{2,4},{1,9},{5,13}... | collective-permute-start | bytes 393224 | tf_op jit(solution)/shard_map/ppermute | solution.py:52
  152.0 30.1 %collective-permute-start.23 = (bf16[128,512]{1,0:T(8,128)(2,1)S(1)}, bf16[128,512]{1,0:T(8,128)(2,1)S(1)}, u32[]{:S(2)}, u32[]{:S(2)}) collective-permute-start(bf16[128,512]{1,0:T(8,128)(2,1)S(1)} %get-tuple-element.27), channel_id=1, source_target_pairs={{0,4},{4,8},{8,12},{12,14},{14,10},{10,6},{6,2},{2,0},{1,5},{5,9},... | collective-permute-start | bytes 393224 | tf_op jit(solution)/shard_map/ppermute | solution.py:52
  152.9 29.4 %collective-permute-start.47 = (bf16[128,1024]{0,1:T(8,128)(2,1)S(1)}, bf16[128,1024]{0,1:T(8,128)(2,1)S(1)}, u32[]{:S(2)}, u32[]{:S(2)}) collective-permute-start(bf16[128,1024]{0,1:T(8,128)(2,1)S(1)} %pad_maximum_fusion.5), channel_id=1, source_target_pairs={{4,0},{8,4},{12,8},{14,12},{10,14},{6,10},{2,6},{0,2},{5,1},{9,5},... | collective-permute-start | bytes 786440 | tf_op jit(solution)/shard_map/ppermute | solution.py:95
  156.4 14.0 %collective-permute-start.43 = (bf16[128,1024]{0,1:T(8,128)(2,1)S(1)}, bf16[128,1024]{0,1:T(8,128)(2,1)S(1)}, u32[]{:S(2)}, u32[]{:S(2)}) collective-permute-start(bf16[128,1024]{0,1:T(8,128)(2,1)S(1)} %pad_maximum_fusion.4), channel_id=1, source_target_pairs={{0,4},{4,8},{8,12},{12,14},{14,10},{10,6},{6,2},{2,0},{1,5},{5,9},... | collective-permute-start | bytes 786440 | tf_op jit(solution)/shard_map/ppermute | solution.py:94
  166.2 20.4 %collective-permute-start.14 = (bf16[128,1024]{0,1:T(8,128)(2,1)S(1)}, bf16[128,1024]{0,1:T(8,128)(2,1)S(1)}, u32[]{:S(2)}, u32[]{:S(2)}) collective-permute-start(bf16[128,1024]{0,1:T(8,128)(2,1)S(1)} %pad_maximum_fusion.3), channel_id=1, source_target_pairs={{4,0},{8,4},{12,8},{14,12},{10,14},{6,10},{2,6},{0,2},{5,1},{9,5},... | collective-permute-start | bytes 786440 | tf_op jit(solution)/shard_map/ppermute | solution.py:95
  170.5 11.7 %collective-permute-start.44 = (bf16[128,1024]{0,1:T(8,128)(2,1)S(1)}, bf16[128,1024]{0,1:T(8,128)(2,1)S(1)}, u32[]{:S(2)}, u32[]{:S(2)}) collective-permute-start(bf16[128,1024]{0,1:T(8,128)(2,1)S(1)} %add_convert_fusion.5), channel_id=1, source_target_pairs={{0,4},{4,8},{8,12},{12,14},{14,10},{10,6},{6,2},{2,0},{1,5},{5,9},... | collective-permute-start | bytes 786440 | tf_op jit(solution)/shard_map/ppermute | solution.py:94
  176.6 10.6 %collective-permute-start.11 = (bf16[128,1024]{0,1:T(8,128)(2,1)S(1)}, bf16[128,1024]{0,1:T(8,128)(2,1)S(1)}, u32[]{:S(2)}, u32[]{:S(2)}) collective-permute-start(bf16[128,1024]{0,1:T(8,128)(2,1)S(1)} %add_convert_fusion.10), channel_id=1, source_target_pairs={{0,4},{4,8},{8,12},{12,14},{14,10},{10,6},{6,2},{2,0},{1,5},{5,9},... | collective-permute-start | bytes 786440 | tf_op jit(solution)/shard_map/ppermute | solution.py:94
  182.1 19.6 %collective-permute-start.24 = (bf16[1024,512]{1,0:T(8,128)(2,1)S(1)}, bf16[1024,512]{1,0:T(8,128)(2,1)S(1)}, u32[]{:S(2)}, u32[]{:S(2)}) collective-permute-start(bf16[1024,512]{1,0:T(8,128)(2,1)S(1)} %constant_dynamic-update-slice_fusion.9), channel_id=1, source_target_pairs={{0,1},{1,0},{2,3},{3,2},{4,5},{5,4},{6,7},{7,6},{8,9},{9,8},{10,11... | collective-permute-start | bytes 3145736 | tf_op jit(solution)/shard_map/ppermute | solution.py:147
  182.4 17.2 %collective-permute-start.48 = (bf16[128,1024]{0,1:T(8,128)(2,1)S(1)}, bf16[128,1024]{0,1:T(8,128)(2,1)S(1)}, u32[]{:S(2)}, u32[]{:S(2)}) collective-permute-start(bf16[128,1024]{0,1:T(8,128)(2,1)S(1)} %get-tuple-element.18), channel_id=1, source_target_pairs={{4,0},{8,4},{12,8},{14,12},{10,14},{6,10},{2,6},{0,2},{5,1},{9,5},... | collective-permute-start | bytes 786440 | tf_op jit(solution)/shard_map/ppermute | solution.py:95
  187.4 12.3 %collective-permute-start.15 = (bf16[128,1024]{0,1:T(8,128)(2,1)S(1)}, bf16[128,1024]{0,1:T(8,128)(2,1)S(1)}, u32[]{:S(2)}, u32[]{:S(2)}) collective-permute-start(bf16[128,1024]{0,1:T(8,128)(2,1)S(1)} %get-tuple-element.37), channel_id=1, source_target_pairs={{4,0},{8,4},{12,8},{14,12},{10,14},{6,10},{2,6},{0,2},{5,1},{9,5},... | collective-permute-start | bytes 786440 | tf_op jit(solution)/shard_map/ppermute | solution.py:95
  196.8 14.0 %collective-permute-start.45 = (bf16[128,1024]{0,1:T(8,128)(2,1)S(1)}, bf16[128,1024]{0,1:T(8,128)(2,1)}, u32[]{:S(2)}, u32[]{:S(2)}) collective-permute-start(bf16[128,1024]{0,1:T(8,128)(2,1)S(1)} %get-tuple-element.17), channel_id=1, source_target_pairs={{0,4},{4,8},{8,12},{12,14},{14,10},{10,6},{6,2},{2,0},{1,5},{5,9},... | collective-permute-start | bytes 786440 | tf_op jit(solution)/shard_map/ppermute | solution.py:94
  197.1 15.8 %collective-permute-start.12 = (bf16[128,1024]{0,1:T(8,128)(2,1)S(1)}, bf16[128,1024]{0,1:T(8,128)(2,1)S(1)}, u32[]{:S(2)}, u32[]{:S(2)}) collective-permute-start(bf16[128,1024]{0,1:T(8,128)(2,1)S(1)} %get-tuple-element.36), channel_id=1, source_target_pairs={{0,4},{4,8},{8,12},{12,14},{14,10},{10,6},{6,2},{2,0},{1,5},{5,9},... | collective-permute-start | bytes 786440 | tf_op jit(solution)/shard_map/ppermute | solution.py:94
  199.7 11.1 %collective-permute-start.49 = (bf16[128,1024]{0,1:T(8,128)(2,1)S(1)}, bf16[128,1024]{0,1:T(8,128)(2,1)}, u32[]{:S(2)}, u32[]{:S(2)}) collective-permute-start(bf16[128,1024]{0,1:T(8,128)(2,1)S(1)} %add_convert_fusion.2), channel_id=1, source_target_pairs={{4,0},{8,4},{12,8},{14,12},{10,14},{6,10},{2,6},{0,2},{5,1},{9,5},... | collective-permute-start | bytes 786440 | tf_op jit(solution)/shard_map/ppermute | solution.py:95
  199.9 13.0 %collective-permute-start.16 = (bf16[128,1024]{0,1:T(8,128)(2,1)S(1)}, bf16[128,1024]{0,1:T(8,128)(2,1)}, u32[]{:S(2)}, u32[]{:S(2)}) collective-permute-start(bf16[128,1024]{0,1:T(8,128)(2,1)S(1)} %add_convert_fusion.7), channel_id=1, source_target_pairs={{4,0},{8,4},{12,8},{14,12},{10,14},{6,10},{2,6},{0,2},{5,1},{9,5},... | collective-permute-start | bytes 786440 | tf_op jit(solution)/shard_map/ppermute | solution.py:95
  (31 other events, 645.0 us)
